TPU v7x, 32 devices: a whole 2x2x4 slice. The times are simulated.
32 devices in a mesh: ep: 32 (over z, y, x, core).
Axes of the slice: x: 2, y: 2, z: 4, core: 2. Of those that a mesh axis runs over, the one named last changes fastest.
Arguments:
- tokens: bfloat16 [576, 2048], P('ep'), may hold values from -6 to 6
- attn_norm_gain: float32 [2048], replicated, may hold values from 0.1 to 1.9
- w_query: bfloat16 [2048, 512], replicated, may hold values from -0.125 to 0.125
- w_key: bfloat16 [2048, 128], replicated, may hold values from -0.125 to 0.125
- w_value: bfloat16 [2048, 128], replicated, may hold values from -0.125 to 0.125
- w_forget: bfloat16 [2048, 8], replicated, may hold values from -0.125 to 0.125
- forget_bias: float32 [8], replicated, may hold values from 0.5 to 4
- w_attn_out: bfloat16 [512, 2048], replicated, may hold values from -0.25 to 0.25
- cache_keys: bfloat16 [576, 1024, 128], P('ep'), may hold values from -72 to 72
- cache_values: bfloat16 [576, 1024, 128], P('ep'), may hold values from -6 to 6
- cache_logcum: float32 [576, 8, 1024], P('ep'), as said below
- cache_lengths: int32 [576], P('ep'), may hold values from 128 to 1024
- expert_norm_gain: float32 [2048], replicated, may hold values from 0.4 to 40
- expert_ids: int32 [576, 6], P('ep'), may hold values from 0 to 31, all different within a row; in each aligned block of 18 rows (0 to 17, 18 to 35, ...) at most 6 rows name the same one
- expert_weights: float32 [576, 6], P('ep'), may hold values from 0.1 to 1
- w_expert_gate: bfloat16 [32, 2048, 512], P('ep'), may hold values from -0.125 to 0.125
- w_expert_up: bfloat16 [32, 2048, 512], P('ep'), may hold values from -0.125 to 0.125
- w_expert_down: bfloat16 [32, 512, 2048], P('ep'), may hold values from -0.25 to 0.25
- w_dense_gate: bfloat16 [2048, 4096], P(None, 'ep'), may hold values from -0.125 to 0.125
- w_dense_up: bfloat16 [2048, 4096], P(None, 'ep'), may hold values from -2 to 2
- w_dense_down: bfloat16 [4096, 2048], P('ep'), may hold values from -0.09375 to 0.09375
- dense_norm_gain: float32 [4096], replicated, may hold values from 0.1 to 1.9
- branch_gate: float32 [2048], replicated, may hold values from -0.125 to 0.125
Outputs:
- result: bfloat16 [576, 2048], P('ep')
Inputs may be any that keep to these rules, and one draw needn't show every extreme that they name: `cache_logcum`: along the positions of each sequence and head the values never rise. `expert_ids`: each row names 6 different experts; among the rows of one device no expert is named by more than 6 rows, and in every draw some device names some expert exactly 6 times.
All inputs are finite; a program needn't handle non-finite values.
Results may differ from a plain program's by a relative error of at most 0.012.
The roundings to bfloat16 on the way count: a program that leaves them out, or rounds other values in their place, can miss the bound.
Values may be sent and summed in bfloat16 or wider, within the bound.
A program may use at most 128 MiB of HBM per device.

v0:
```python
import functools

import jax
import jax.numpy as jnp
from jax import lax
from jax.experimental import pallas as pl
from jax.experimental.pallas import tpu as pltpu
from jax.sharding import PartitionSpec as P

HEADS = 8
KV_HEADS = 2
HEAD_DIM = 64
TOPK = 6


EPS = 1e-06
LIMIT = 7.0
ALPHA = 1.702


def normalize(values, gain):
    return values * lax.rsqrt(jnp.mean(values * values, axis=-1, keepdims=True) + EPS) * gain


def stored(values):
    return lax.optimization_barrier(values.astype(jnp.bfloat16))


def front_body(
    lengths,
    tokens,
    gain_ref,
    w_query,
    w_key,
    w_value,
    w_forget,
    bias,
    w_out,
    gain_next,
    keys,
    values,
    logcum,
    mixed_ref,
    routed_ref,
    query_s,
    key_s,
    value_s,
    forget_s,
    attended_s,
):
    step = pl.program_id(0)
    batch, length, pair = keys.shape
    rows = jnp.float32
    group = HEADS // KV_HEADS
    tiles = HEADS * HEAD_DIM // pair

    @pl.when(step == 0)
    def _():
        normed = normalize(tokens[...].astype(rows), gain_ref[...]).astype(jnp.bfloat16)
        for weight, kept in ((w_key, key_s), (w_value, value_s)):
            product = jnp.dot(normed, weight[...], preferred_element_type=rows)
            kept[...] = product.astype(jnp.bfloat16).astype(rows)
        product = jnp.dot(normed, w_query[...], preferred_element_type=rows)
        product = product.astype(jnp.bfloat16).astype(rows)
        for tile in range(tiles):
            query_s[tile] = product[:, tile * pair : (tile + 1) * pair]
        forget = lax.dot_general(
            w_forget[...], normed, (((1,), (1,)), ((), ())), preferred_element_type=rows
        )
        forget = forget + bias[...]
        forget_s[...] = jnp.minimum(forget, 0.0) - jnp.log1p(jnp.exp(-jnp.abs(forget)))

    lane = lax.broadcasted_iota(jnp.int32, (HEADS, pair), 1)
    head = lax.broadcasted_iota(jnp.int32, (HEADS, pair), 0)
    odd = lane // HEAD_DIM
    place = head // group
    seq_lane = lax.broadcasted_iota(jnp.int32, forget_s.shape, 1)
    position = lax.broadcasted_iota(jnp.int32, (HEADS, length), 1)
    scale = HEAD_DIM ** (-0.5)
    for item in range(batch):
        seq = step * batch + item
        stay = jnp.zeros((HEADS, pair), rows)
        move = jnp.zeros((HEADS, pair), rows)
        for tile in range(tiles):
            piece = jnp.broadcast_to(
                query_s[tile, pl.ds(seq, 1), :], (HEADS, pair)
            )
            own_lanes = head == 2 * tile + odd
            stay = jnp.where(own_lanes & (odd == place), piece, stay)
            move = jnp.where(own_lanes & (odd != place), piece, move)
        query = stay + pltpu.roll(move, HEAD_DIM, 1)
        own = jnp.sum(query * key_s[pl.ds(seq, 1), :], axis=1, keepdims=True) * scale
        forget = jnp.sum(jnp.where(seq_lane == seq, forget_s[...], 0.0), axis=1, keepdims=True)
        cum = logcum[item]
        live_count = lengths[seq]
        last = jnp.sum(jnp.where(position == live_count - 1, cum, 0.0), axis=1, keepdims=True)
        scores = lax.dot_general(
            query.astype(jnp.bfloat16),
            keys[item],
            (((1,), (1,)), ((), ())),
            preferred_element_type=rows,
        )
        scores = scores * scale + ((last + forget) - cum)
        scores = jnp.where(position < live_count, scores, -jnp.inf)
        top = jnp.maximum(jnp.max(scores, axis=1, keepdims=True), own)
        expo = jnp.exp(scores - top)
        own_expo = jnp.exp(own - top)
        total = jnp.sum(expo, axis=1, keepdims=True) + own_expo
        weights = (expo / total).astype(jnp.bfloat16)
        own_weight = (own_expo / total).astype(jnp.bfloat16).astype(rows)
        out = jnp.dot(weights, values[item], preferred_element_type=rows)
        out = out + own_weight * value_s[pl.ds(seq, 1), :]
        turned = pltpu.roll(out, HEAD_DIM, 1)
        for tile in range(tiles):
            own_lanes = head == 2 * tile + odd
            part = jnp.where(own_lanes, jnp.where(odd == place, out, turned), 0.0)
            attended_s[tile, pl.ds(seq, 1), :] = jnp.sum(part, axis=0, keepdims=True)

    @pl.when(step == pl.num_programs(0) - 1)
    def _():
        attended = jnp.concatenate([attended_s[tile] for tile in range(tiles)], axis=1)
        attended = attended.astype(jnp.bfloat16)
        mixed = tokens[...].astype(rows) + jnp.dot(
            attended, w_out[...], preferred_element_type=rows
        )
        mixed = mixed.astype(jnp.bfloat16)
        mixed_ref[...] = mixed
        routed_ref[...] = normalize(mixed.astype(rows), gain_next[...]).astype(jnp.bfloat16)


def front(
    tokens, gain, w_query, w_key, w_value, w_forget, bias, w_out, keys, values, logcum, lengths, gain_next
):
    seqs, width = tokens.shape
    batch = max(size for size in (1, 2, 3) if seqs % size == 0)
    pair = keys.shape[2]

    def whole(*shape):
        return pl.BlockSpec(shape, lambda i, *_: (0,) * len(shape))

    def each(*shape):
        return pl.BlockSpec((batch, *shape), lambda i, *_: (i, 0, 0))

    small = (
        tokens,
        gain[None, :],
        w_query,
        w_key,
        w_value,
        w_forget.T,
        bias[:, None],
        w_out,
        gain_next[None, :],
    )
    kept = jax.ShapeDtypeStruct((seqs, width), jnp.bfloat16)
    return pl.pallas_call(
        front_body,
        out_shape=(kept, kept),
        grid_spec=pltpu.PrefetchScalarGridSpec(
            num_scalar_prefetch=1,
            grid=(seqs // batch,),
            in_specs=[whole(*array.shape) for array in small]
            + [each(*keys.shape[1:]), each(*values.shape[1:]), each(*logcum.shape[1:])],
            out_specs=[whole(seqs, width)] * 2,
            scratch_shapes=[
                pltpu.VMEM((HEADS * HEAD_DIM // pair, seqs, pair), jnp.float32),
                pltpu.VMEM((seqs, pair), jnp.float32),
                pltpu.VMEM((seqs, pair), jnp.float32),
                pltpu.VMEM((HEADS, seqs), jnp.float32),
                pltpu.VMEM((HEADS * HEAD_DIM // pair, seqs, pair), jnp.float32),
            ],
        ),
        compiler_params=pltpu.CompilerParams(
            dimension_semantics=("arbitrary",), vmem_limit_bytes=40 * 1024 * 1024
        ),
        cost_estimate=pl.CostEstimate(
            flops=10**9, bytes_accessed=16 * 10**6, transcendentals=2 * 10**5
        ),
        name="front",
    )(lengths, *small, keys, values, logcum)


def split3(values):
    parts = []
    for _ in range(3):
        part = stored(values)
        parts.append(part)
        values = values - part.astype(jnp.float32)
    return parts


def expert_unit(rows, gate_w, up_w, down_w):
    gate = jnp.minimum(jnp.dot(rows, gate_w, preferred_element_type=jnp.float32), LIMIT)
    up = jnp.clip(jnp.dot(rows, up_w, preferred_element_type=jnp.float32), -LIMIT, LIMIT)
    act = ((up + 1.0) * gate * jax.nn.sigmoid(gate * ALPHA)).astype(jnp.bfloat16)
    return jnp.dot(act, down_w, preferred_element_type=jnp.float32).astype(jnp.bfloat16)


def reach(source, target, sent, landed, device):
    return pltpu.make_async_remote_copy(
        src_ref=source,
        dst_ref=target,
        send_sem=sent,
        recv_sem=landed,
        device_id=(device,),
        device_id_type=pl.DeviceIdType.MESH,
    )


def to_row(column, same):
    return jnp.sum(jnp.where(same, column, 0.0), axis=0, keepdims=True)


def to_column(row, same):
    return jnp.sum(jnp.where(same, row, 0.0), axis=1, keepdims=True)


def rest_body(
    units_total,
    plane,
    packed,
    mixed,
    w_gate,
    w_up,
    w_down,
    d_gate,
    d_up,
    d_down,
    gain,
    branch,
    out,
    rows_s,
    units_s,
    answer_s,
    coef_s,
    square_s,
    squares_s,
    theirs_s,
    joint_s,
    final_s,
    own_sem,
    ag_send,
    ag_recv,
    fw_send,
    fw_recv,
    sq_send,
    sq_recv,
    d2d_send,
    d2d_recv,
    rs_send,
    rs_recv,
):
    kind = jnp.float32
    n = squares_s.shape[0]
    chips = n // 2
    pad = packed.shape[0]
    width = out.shape[1]
    chunk = units_s.shape[1] // pad
    halves = chips // chunk
    size = chunk * pad
    me = lax.axis_index("ep")
    core = lax.rem(me, 2)
    chip = me // 2
    other = chip * 2 + 1 - core
    mine = core * chips
    peer = (1 - core) * chips

    barrier = pltpu.get_barrier_semaphore()

    @pl.loop(1, n)
    def _(k):
        pl.semaphore_signal(
            barrier,
            inc=1,
            device_id=(lax.rem(me + k, n),),
            device_id_type=pl.DeviceIdType.MESH,
        )

    pl.semaphore_wait(barrier, n - 1)

    deep = chips // plane
    level = chip // plane
    spot = lax.rem(chip, plane)

    def before(dz, dp):
        return lax.rem(level - dz + deep, deep) * plane + lax.rem(spot - dp + plane, plane)

    def along(dz):
        to = lax.rem(level + dz, deep) * plane + spot
        k = dz * plane
        return reach(packed, rows_s.at[mine + chip], ag_send.at[k], ag_recv.at[k], to * 2 + core)

    def across(dz, dp):
        to = level * plane + lax.rem(spot + dp, plane)
        k = dz * plane + dp
        slot = rows_s.at[mine + before(dz, 0)]
        return reach(slot, slot, ag_send.at[k], ag_recv.at[k], to * 2 + core)

    def landed(dz, dp):
        slot = rows_s.at[mine + before(dz, dp)]
        k = dz * plane + dp
        return reach(slot, slot, ag_send.at[k], ag_recv.at[k], before(0, dp) * 2 + core)

    def forward(dz, dp):
        slot = rows_s.at[mine + before(dz, dp)]
        k = dz * plane + dp
        return reach(slot, slot, fw_send.at[k], fw_recv.at[k], other)

    def forwarded(dz, dp):
        slot = rows_s.at[peer + before(dz, dp)]
        k = dz * plane + dp
        return reach(slot, slot, fw_send.at[k], fw_recv.at[k], other)

    keep = pltpu.make_async_copy(packed, rows_s.at[mine + chip], own_sem)
    keep.start()

    @pl.loop(1, deep)
    def _(dz):
        along(dz).start()

    keep.wait()

    @pl.loop(1, plane)
    def _(dp):
        across(0, dp).start()

    forward(0, 0).start()

    @pl.loop(1, deep)
    def _(dz):
        landed(dz, 0).wait_recv()

        @pl.loop(1, plane)
        def _(dp):
            across(dz, dp).start()

        forward(dz, 0).start()

    @pl.loop(0, deep)
    def _(dz):
        @pl.loop(1, plane)
        def _(dp):
            landed(dz, dp).wait_recv()
            forward(dz, dp).start()

    @pl.loop(0, deep)
    def _(dz):
        @pl.loop(0, plane)
        def _(dp):
            forwarded(dz, dp).wait_recv()

    first = lax.broadcasted_iota(jnp.int32, (size, size), 0)
    second = lax.broadcasted_iota(jnp.int32, (size, size), 1)
    same = first == second

    def load(at):
        block = rows_s[pl.ds(at * chunk, chunk)]
        return block.astype(kind).reshape(size, block.shape[2])

    @pl.loop(0, 2 * halves)
    def _(at):
        wide = load(at)
        block = wide[:, :width].astype(jnp.bfloat16)
        gate = jnp.dot(block, d_gate[...], preferred_element_type=kind)
        up = jnp.dot(block, d_up[...], preferred_element_type=kind)
        units = (gate * jax.nn.sigmoid(gate) * up).astype(jnp.bfloat16).astype(kind)
        units_s[at] = units
        square_s[at] = to_row(jnp.sum(units * units, axis=1, keepdims=True), same)
        side = wide[:, width:]
        lane = lax.broadcasted_iota(jnp.int32, side.shape, 1)
        picked = jnp.where((side == me.astype(kind)) & (lane < TOPK), 1.0, 0.0)
        weight = jnp.zeros((size, 1), kind)
        for part in (3, 2, 1):
            moved = pltpu.roll(side, side.shape[1] - part * TOPK, 1)
            weight = weight + jnp.sum(picked * moved, axis=1, keepdims=True)
        branch_scale = jax.nn.sigmoid(
            jnp.sum(wide[:, :width] * branch[...], axis=1, keepdims=True)
        )
        coef_s[at] = jnp.where(lane == 0, weight, branch_scale)

    def share(k):
        return reach(
            square_s, squares_s.at[k], sq_send.at[k], sq_recv.at[k], lax.rem(me + k, n)
        )

    @pl.loop(1, n)
    def _(k):
        share(k).start()

    @pl.loop(0, 2 * halves)
    def _(at):
        block = load(at)[:, :width].astype(jnp.bfloat16)
        answer_s[at] = expert_unit(block, w_gate[...], w_up[...], w_down[...])

    @pl.loop(1, n)
    def _(k):
        share(k).wait_recv()

    squares_s[0] = square_s[...]
    totals = jnp.sum(squares_s[...], axis=0)
    square_rows = lax.rsqrt(totals / units_total + EPS)
    squares_s[0] = square_rows

    def partial(at):
        scale = to_column(squares_s[0, at], same)
        hidden = (units_s[at] * scale * gain[...]).astype(jnp.bfloat16)
        dense = jnp.dot(hidden, d_down[...], preferred_element_type=kind)
        coef = coef_s[at]
        routed = coef[:, 0:1] * answer_s[at].astype(kind)
        return (routed + coef[:, 1:2] * dense).reshape(chunk, pad, width)

    def cross(half):
        part = pl.ds(half * chunk, chunk)
        return reach(theirs_s.at[part], joint_s.at[part], d2d_send.at[half], d2d_recv.at[half], other)

    def back(dz, dp):
        k = dz * plane + dp
        slot = joint_s.at[before(dz, dp)]
        return reach(slot, final_s.at[k], rs_send.at[k], rs_recv.at[k], before(0, dp) * 2 + core)

    def down(dz):
        k = dz * plane
        to = before(dz, 0)
        return reach(joint_s.at[to], final_s.at[k], rs_send.at[k], rs_recv.at[k], to * 2 + core)

    def collected(dz):
        total = joint_s[before(dz, 0)].astype(kind)
        for dp in range(1, plane):
            back(dz, dp).wait_recv()
            total = total + final_s[dz * plane + dp].astype(kind)
        return total

    @pl.loop(0, halves)
    def _(half):
        theirs_s[pl.ds(half * chunk, chunk)] = partial((1 - core) * halves + half).astype(
            jnp.bfloat16
        )
        cross(half).start()

    @pl.loop(0, halves)
    def _(half):
        part = pl.ds(half * chunk, chunk)
        own = partial(core * halves + half)
        cross(half).wait_recv()
        joint_s[part] = (own + joint_s[part].astype(kind)).astype(jnp.bfloat16)

    @pl.loop(1, deep + 1)
    def _(step):
        @pl.loop(1, plane)
        def _(dp):
            back(lax.rem(step, deep), dp).start()

    @pl.loop(1, deep)
    def _(dz):
        joint_s[before(dz, 0)] = collected(dz).astype(jnp.bfloat16)
        down(dz).start()

    total = collected(0)
    for dz in range(1, deep):
        down(dz).wait_recv()
        total = total + final_s[dz * plane].astype(kind)
    result = mixed[...].astype(kind) + total[: mixed.shape[0]]
    out[...] = result.astype(jnp.bfloat16)

    @pl.loop(1, deep)
    def _(dz):
        along(dz).wait_send()
        down(dz).wait_send()

    @pl.loop(0, deep)
    def _(dz):
        forward(dz, 0).wait_send()

        @pl.loop(1, plane)
        def _(dp):
            across(dz, dp).wait_send()
            back(dz, dp).wait_send()
            forward(dz, dp).wait_send()

    @pl.loop(1, n)
    def _(k):
        share(k).wait_send()

    @pl.loop(0, halves)
    def _(half):
        cross(half).wait_send()


def rest(n, packed, mixed, w_gate, w_up, w_down, d_gate, d_up, d_down, gain, branch, units_total):
    pad = packed.shape[0]
    width = mixed.shape[1]
    local = d_gate.shape[1]
    chips = n // 2
    chunk = max(size for size in (1, 2, 4, 8) if chips % size == 0)
    halves = chips // chunk
    plane = chips // 4 if chips % 4 == 0 else chips
    size = chunk * pad
    half_type = jnp.bfloat16
    vmem = pl.BlockSpec(memory_space=pltpu.VMEM)
    dma = pltpu.SemaphoreType.DMA
    return pl.pallas_call(
        functools.partial(rest_body, units_total, plane),
        out_shape=jax.ShapeDtypeStruct(mixed.shape, half_type),
        in_specs=[vmem] * 10,
        out_specs=vmem,
        scratch_shapes=[
            pltpu.VMEM((n, *packed.shape), half_type),
            pltpu.VMEM((2 * halves, size, local), jnp.float32),
            pltpu.VMEM((2 * halves, size, width), half_type),
            pltpu.VMEM((2 * halves, size, 128), jnp.float32),
            pltpu.VMEM((2 * halves, 1, size), jnp.float32),
            pltpu.VMEM((n, 2 * halves, 1, size), jnp.float32),
            pltpu.VMEM((chips, pad, width), half_type),
            pltpu.VMEM((chips, pad, width), half_type),
            pltpu.VMEM((chips, pad, width), half_type),
            dma,
            dma((chips,)),
            dma((chips,)),
            dma((chips,)),
            dma((chips,)),
            dma((n,)),
            dma((n,)),
            dma((halves,)),
            dma((halves,)),
            dma((chips,)),
            dma((chips,)),
        ],
        compiler_params=pltpu.CompilerParams(
            collective_id=0, has_side_effects=True, vmem_limit_bytes=62 * 1024 * 1024
        ),
        name="rest",
    )(packed, mixed, w_gate, w_up, w_down, d_gate, d_up, d_down, gain, branch)


def shards(
    tokens,
    attn_norm_gain,
    w_query,
    w_key,
    w_value,
    w_forget,
    forget_bias,
    w_attn_out,
    cache_keys,
    cache_values,
    cache_logcum,
    cache_lengths,
    expert_norm_gain,
    expert_ids,
    expert_weights,
    w_expert_gate,
    w_expert_up,
    w_expert_down,
    w_dense_gate,
    w_dense_up,
    w_dense_down,
    dense_norm_gain,
    branch_gate,
):
    mixed, routed_in = front(
        tokens,
        attn_norm_gain,
        w_query,
        w_key,
        w_value,
        w_forget,
        forget_bias,
        w_attn_out,
        cache_keys,
        cache_values,
        cache_logcum,
        cache_lengths,
        expert_norm_gain,
    )
    n = lax.axis_size("ep")
    me = lax.axis_index("ep")
    seqs = tokens.shape[0]
    extra = jnp.concatenate([expert_ids.astype(jnp.bfloat16), *split3(expert_weights)], axis=1)
    packed = jnp.concatenate([routed_in, jnp.pad(extra, ((0, 0), (0, 128 - 4 * TOPK)))], axis=1)
    packed = jnp.pad(packed, ((0, -seqs % 8), (0, 0)))
    local = w_dense_gate.shape[1]
    gain = lax.dynamic_slice_in_dim(dense_norm_gain, me * local, local, 0)
    return rest(
        n,
        packed,
        mixed,
        w_expert_gate[0],
        w_expert_up[0],
        w_expert_down[0],
        w_dense_gate,
        w_dense_up,
        w_dense_down,
        gain[None, :],
        branch_gate[None, :],
        dense_norm_gain.shape[0],
    )


def solution(mesh):
    in_specs = (
        P("ep", None),
        P(),
        P(),
        P(),
        P(),
        P(),
        P(),
        P(),
        P("ep", None, None),
        P("ep", None, None),
        P("ep", None, None),
        P("ep"),
        P(),
        P("ep", None),
        P("ep", None),
        P("ep", None, None),
        P("ep", None, None),
        P("ep", None, None),
        P(None, "ep"),
        P(None, "ep"),
        P("ep", None),
        P(),
        P(),
    )
    out_specs = P("ep", None)
    return jax.shard_map(shards, mesh=mesh, in_specs=in_specs, out_specs=out_specs, check_vma=False)
```

profile of v0, /device:TPU:0, one launch (start us, length us, event | category | flops | bytes accessed | tf_op | source)
XLA Modules:
  0.0 99.6 jit_solution(5491594527085155684)
XLA Ops:
  0.0 0.7 convert_element_type.23
  0.7 0.1 copy.32
  0.8 0.8 copy.30
  1.6 0.7 convert_element_type.22
  2.3 0.1 copy.31
  2.4 0.1 fusion.10
  2.5 0.7 copy.28.bias
  3.2 2.3 %copy-done.1 = bf16[18,1024,128]{2,1,0:T(8,128)(2,1)S(1)} copy-done((bf16[18,1024,128]{2,1,0:T(8,128)(2,1)S(1)}, bf16[18,1024,128]{2,1,0:T(8,128)(2,1)}, u32[]{:S(2)}) %copy-start.1) | copy-done | bytes 4718616
  5.6 1.6 %copy-done.2 = bf16[2048,512]{1,0:T(8,128)(2,1)S(1)} copy-done((bf16[2048,512]{1,0:T(8,128)(2,1)S(1)}, bf16[2048,512]{1,0:T(8,128)(2,1)}, u32[]{:S(2)}) %copy-start.2) | copy-done | bytes 2097176
  7.2 1.6 %copy-done.3 = bf16[512,2048]{1,0:T(8,128)(2,1)S(1)} copy-done((bf16[512,2048]{1,0:T(8,128)(2,1)S(1)}, bf16[512,2048]{1,0:T(8,128)(2,1)}, u32[]{:S(2)}) %copy-start.3) | copy-done | bytes 2097176
  8.8 1.1 %copy-done.4 = f32[18,8,1024]{2,1,0:T(8,128)S(1)} copy-done((f32[18,8,1024]{2,1,0:T(8,128)S(1)}, f32[18,8,1024]{2,1,0:T(8,128)}, u32[]{:S(2)}) %copy-start.4) | copy-done | bytes 589848
  9.8 1.0 %copy-done.5 = bf16[2048,128]{1,0:T(8,128)(2,1)S(1)} copy-done((bf16[2048,128]{1,0:T(8,128)(2,1)S(1)}, bf16[2048,128]{1,0:T(8,128)(2,1)}, u32[]{:S(2)}) %copy-start.5) | copy-done | bytes 524312
  10.9 1.0 %copy-done.6 = bf16[2048,128]{1,0:T(8,128)(2,1)S(1)} copy-done((bf16[2048,128]{1,0:T(8,128)(2,1)S(1)}, bf16[2048,128]{1,0:T(8,128)(2,1)}, u32[]{:S(2)}) %copy-start.6) | copy-done | bytes 524312
  11.9 0.9 copy-done.7
  12.8 0.8 copy-done.9
  13.6 0.7 copy-done.10
  14.3 0.7 copy-done.11
  15.0 0.7 copy-done.12
  15.6 11.4 %front.1 = (bf16[18,2048]{1,0:T(8,128)(2,1)S(1)}, bf16[18,2048]{1,0:T(8,128)(2,1)S(1)}) custom-call(s32[18]{0:T(128)S(1)} %copy-done.12, bf16[18,2048]{1,0:T(8,128)(2,1)S(1)} %copy-done.7, f32[1,2048]{1,0:T(1,128)S(1)} %bitcast.11, bf16[2048,512]{1,0:T(8,128)(2,1)S(1)} %copy-done.2, bf16[2048,128]{1,0:T(8,128)(2,1)S(1)} %copy-done.5, ...), custom_call_target="tpu_custom_call" | custom-call | flops 1000000000 | bytes 16000000 | tf_op jit(solution)/shard_map/front/pallas_call | solution.py:156
  27.0 0.6 copy-done.8
  27.6 0.6 fusion.2.packed
  28.3 0.6 dynamic-slice_bitcast_fusion.gain
  28.9 69.2 %rest.1 = bf16[18,2048]{1,0:T(8,128)(2,1)} custom-call(bf16[24,2176]{1,0:T(8,128)(2,1)} %fusion.2.packed, bf16[18,2048]{1,0:T(8,128)(2,1)} %copy-done.8, bf16[2048,512]{1,0:T(8,128)(2,1)} %bitcast.13, bf16[2048,512]{1,0:T(8,128)(2,1)} %bitcast.14, bf16[512,2048]{1,0:T(8,128)(2,1)} %bitcast.15, bf16[2048,128]{1,0:T(8,128)(2,1)} %d_gate.1, ...), custom_call_target="tpu_custom_call" | custom-call | tf_op jit(solution)/shard_map/rest/pallas_call | solution.py:501
  98.0 1.5 %copy.34 = bf16[18,2048]{1,0:T(8,128)(2,1)} copy(bf16[18,2048]{1,0:T(8,128)(2,1)} %rest.1) | data formatting | bytes 147456
  (16 shorter events, 0.0 us)
Async XLA Ops:
  0.0 28.3 %copy-start = (f32[4096]{0:T(1024)S(1)}, f32[4096]{0:T(1024)}, u32[]{:S(2)}) copy-start(f32[4096]{0:T(1024)} %param.44) | copy-start | bytes 49156
  3.2 2.3 %copy-start.1 = (bf16[18,1024,128]{2,1,0:T(8,128)(2,1)S(1)}, bf16[18,1024,128]{2,1,0:T(8,128)(2,1)}, u32[]{:S(2)}) copy-start(bf16[18,1024,128]{2,1,0:T(8,128)(2,1)} %keys.1) | copy-start | bytes 14155780
  5.6 1.6 %copy-start.2 = (bf16[2048,512]{1,0:T(8,128)(2,1)S(1)}, bf16[2048,512]{1,0:T(8,128)(2,1)}, u32[]{:S(2)}) copy-start(bf16[2048,512]{1,0:T(8,128)(2,1)} %w_query.1) | copy-start | bytes 6291460
  7.2 1.6 %copy-start.3 = (bf16[512,2048]{1,0:T(8,128)(2,1)S(1)}, bf16[512,2048]{1,0:T(8,128)(2,1)}, u32[]{:S(2)}) copy-start(bf16[512,2048]{1,0:T(8,128)(2,1)} %w_out.1) | copy-start | bytes 6291460
  8.8 1.1 %copy-start.4 = (f32[18,8,1024]{2,1,0:T(8,128)S(1)}, f32[18,8,1024]{2,1,0:T(8,128)}, u32[]{:S(2)}) copy-start(f32[18,8,1024]{2,1,0:T(8,128)} %logcum.1) | copy-start | bytes 1769476
  9.8 1.0 %copy-start.5 = (bf16[2048,128]{1,0:T(8,128)(2,1)S(1)}, bf16[2048,128]{1,0:T(8,128)(2,1)}, u32[]{:S(2)}) copy-start(bf16[2048,128]{1,0:T(8,128)(2,1)} %w_key.1) | copy-start | bytes 1572868
  10.9 1.0 %copy-start.6 = (bf16[2048,128]{1,0:T(8,128)(2,1)S(1)}, bf16[2048,128]{1,0:T(8,128)(2,1)}, u32[]{:S(2)}) copy-start(bf16[2048,128]{1,0:T(8,128)(2,1)} %w_value.1) | copy-start | bytes 1572868
  11.9 0.9 copy-start.7
  12.8 0.8 copy-start.9
  13.6 0.7 copy-start.10
  14.3 0.7 copy-start.11
  15.0 0.7 copy-start.12
  27.0 0.6 copy-start.8
where the time goes:
time: 100 us; the launch traced here: 99.6 us
  Pallas kernels  80.5 us (80%)
  local copies, waits for them, and re-layouts  16.9 us (17%)
  other arithmetic  2.14 us (2%)
    pallas_call x1, Pallas kernels, rest(): pl.pallas_call(functools.partial(rest_body, units_total, plane), out_shap...  69.2 us
    unnamed x28, local copies, waits for them, and re-layouts  15.3 us
    pallas_call x1, Pallas kernels, front(): pl.pallas_call(front_body, out_shape=(kept, kept), grid_spec=pltpu.Prefet...  11.4 us

commit v1 on v0

--- a/solution.py
+++ b/solution.py
@@ -532,6 +532,792 @@
     )(packed, mixed, w_gate, w_up, w_down, d_gate, d_up, d_down, gain, branch)
 
 
+def fast_body(
+    units_total,
+    tokens_h,
+    gain_h,
+    w_query_h,
+    w_key_h,
+    w_value_h,
+    w_forget_h,
+    bias_h,
+    w_out_h,
+    keys_h,
+    values_h,
+    logcum_h,
+    lengths_h,
+    gain_next_h,
+    ids_h,
+    weights_h,
+    e_gate_h,
+    e_up_h,
+    e_down_h,
+    d_gate_h,
+    d_up_h,
+    d_down_h,
+    d_gain_h,
+    branch_h,
+    out,
+    tokens_s,
+    gain_s,
+    w_qkv_s,
+    w_forget_s,
+    bias_s,
+    w_out_s,
+    keys_s,
+    values_s,
+    logcum_s,
+    lengths_s,
+    gain_next_s,
+    ids_s,
+    weights_s,
+    e_gate_s,
+    e_up_s,
+    e_down_s,
+    d_in_s,
+    d_down_s,
+    d_gain_s,
+    branch_s,
+    query_s,
+    key_s,
+    value_s,
+    forget_s,
+    own_s,
+    heads_s,
+    mixed_s,
+    fold_s,
+    rows_s,
+    x_s,
+    spread_s,
+    hidden_s,
+    branch_col_s,
+    square_s,
+    squares_s,
+    info_s,
+    infos_s,
+    scale_s,
+    coef_s,
+    answer_s,
+    part_s,
+    joint_s,
+    pair_s,
+    first_a,
+    first_b,
+    turn_a,
+    turn_b,
+    second_a,
+    second_b,
+    level_s,
+    levels_s,
+    ld,
+    kv_sem,
+    z_send,
+    z_recv,
+    x_send,
+    x_recv,
+    y_send,
+    y_recv,
+    da_send,
+    da_recv,
+    db_send,
+    db_recv,
+    f_send,
+    f_recv,
+    i_send,
+    i_recv,
+    q_send,
+    q_recv,
+    c_send,
+    c_recv,
+    s1a_send,
+    s1a_recv,
+    s1b_send,
+    s1b_recv,
+    s2a_send,
+    s2a_recv,
+    s2b_send,
+    s2b_recv,
+    zz_send,
+    zz_recv,
+):
+    kind = jnp.float32
+    half_type = jnp.bfloat16
+    n = squares_s.shape[0]
+    chips = n // 2
+    deep = x_s.shape[0]
+    plane = chips // deep
+    side = 2
+    seqs, width = tokens_s.shape
+    block, wide = rows_s.shape[1:]
+    cut = wide // 2
+    fold = wide - width
+    folds = width // fold
+    spare = seqs - block
+    members = 2 * plane
+    bulk = members * block
+    tail = members * spare
+    length, pair = keys_s.shape[1:]
+    group = HEADS // KV_HEADS
+    tiles = HEADS * HEAD_DIM // pair
+    me = lax.axis_index("ep")
+    core = lax.rem(me, 2)
+    chip = me // 2
+    other = chip * 2 + 1 - core
+    level = chip // plane
+    spot = lax.rem(chip, plane)
+    row = spot // side
+    col = lax.rem(spot, side)
+
+    barrier = pltpu.get_barrier_semaphore()
+
+    @pl.loop(1, n)
+    def _(k):
+        pl.semaphore_signal(
+            barrier,
+            inc=1,
+            device_id=(lax.rem(me + k, n),),
+            device_id_type=pl.DeviceIdType.MESH,
+        )
+
+    heads_wide = HEADS * HEAD_DIM
+    loads = [
+        (tokens_h, tokens_s),
+        (gain_h, gain_s),
+        (w_query_h, w_qkv_s.at[:, 0:heads_wide]),
+        (w_key_h, w_qkv_s.at[:, heads_wide : heads_wide + pair]),
+        (w_value_h, w_qkv_s.at[:, heads_wide + pair : heads_wide + 2 * pair]),
+        (w_forget_h, w_forget_s),
+        (bias_h, bias_s),
+        (lengths_h, lengths_s),
+        (logcum_h, logcum_s),
+        (ids_h, ids_s),
+        (weights_h, weights_s),
+    ]
+    later = [
+        (w_out_h, w_out_s),
+        (gain_next_h, gain_next_s),
+        (d_gate_h, d_in_s.at[:, 0:pair]),
+        (d_up_h, d_in_s.at[:, pair : 2 * pair]),
+        (d_gain_h, d_gain_s),
+        (branch_h, branch_s),
+        (e_gate_h.at[0], e_gate_s),
+        (e_up_h.at[0], e_up_s),
+        (e_down_h.at[0], e_down_s),
+        (d_down_h, d_down_s),
+    ]
+    copies = [
+        pltpu.make_async_copy(source, target, ld.at[at])
+        for at, (source, target) in enumerate(loads + later)
+    ]
+    batch = seqs // kv_sem.shape[1]
+    groups = kv_sem.shape[1]
+
+    def cached(at):
+        part = pl.ds(at * batch, batch)
+        return (
+            pltpu.make_async_copy(keys_h.at[part], keys_s.at[part], kv_sem.at[0, at]),
+            pltpu.make_async_copy(values_h.at[part], values_s.at[part], kv_sem.at[1, at]),
+        )
+
+    for copy in copies[: len(loads)]:
+        copy.start()
+
+    @pl.loop(0, groups)
+    def _(at):
+        for copy in cached(at):
+            copy.start()
+
+    for copy in copies[len(loads) :]:
+        copy.start()
+
+    for at in range(9):
+        copies[at].wait()
+
+    normed = normalize(tokens_s[...].astype(kind), gain_s[...]).astype(half_type)
+    product = jnp.dot(normed, w_qkv_s[...], preferred_element_type=kind)
+    product = product.astype(half_type).astype(kind)
+    key_s[...] = product[:, heads_wide : heads_wide + pair]
+    value_s[...] = product[:, heads_wide + pair : heads_wide + 2 * pair]
+    lane = lax.broadcasted_iota(jnp.int32, (seqs, pair), 1)
+    for head in range(HEADS):
+        piece = product[:, head // 2 * pair : (head // 2 + 1) * pair]
+        if head % 2 != head // group:
+            piece = pltpu.roll(piece, HEAD_DIM, 1)
+        piece = jnp.where(lane // HEAD_DIM == head // group, piece, 0.0)
+        query_s[pl.ds(head, seqs, stride=HEADS), :] = piece
+    forget = lax.dot_general(
+        w_forget_s[...], normed, (((1,), (1,)), ((), ())), preferred_element_type=kind
+    )
+    eye = lax.broadcasted_iota(jnp.int32, (HEADS, HEADS), 0)
+    eye = eye == lax.broadcasted_iota(jnp.int32, (HEADS, HEADS), 1)
+    forget = forget + to_column(bias_s[...], eye)
+    forget_s[...] = jnp.minimum(forget, 0.0) - jnp.log1p(jnp.exp(-jnp.abs(forget)))
+
+    seq_lane = lax.broadcasted_iota(jnp.int32, forget_s.shape, 1)
+    position = lax.broadcasted_iota(jnp.int32, (HEADS, length), 1)
+    unit = HEAD_DIM ** (-0.5)
+
+    @pl.loop(0, groups)
+    def _(at):
+        for copy in cached(at):
+            copy.wait()
+        scores_all = []
+        own_all = []
+        for item in range(batch):
+            seq = at * batch + item
+            query = query_s[pl.ds(pl.multiple_of(seq * HEADS, HEADS), HEADS), :]
+            own = jnp.sum(query * key_s[pl.ds(seq, 1), :], axis=1, keepdims=True) * unit
+            forget = jnp.sum(jnp.where(seq_lane == seq, forget_s[...], 0.0), axis=1, keepdims=True)
+            cum = logcum_s[seq]
+            live = lengths_s[seq]
+            last = jnp.sum(jnp.where(position == live - 1, cum, 0.0), axis=1, keepdims=True)
+            scores = lax.dot_general(
+                query.astype(half_type),
+                keys_s[seq],
+                (((1,), (1,)), ((), ())),
+                preferred_element_type=kind,
+            )
+            scores = scores * unit + ((last + forget) - cum)
+            scores_all.append(jnp.where(position < live, scores, -jnp.inf))
+            own_all.append(own)
+        scores = jnp.concatenate(scores_all, axis=0)
+        own = jnp.concatenate(own_all, axis=0)
+        top = jnp.maximum(jnp.max(scores, axis=1, keepdims=True), own)
+        expo = jnp.exp(scores - top)
+        own_expo = jnp.exp(own - top)
+        total = jnp.sum(expo, axis=1, keepdims=True) + own_expo
+        share = (expo / total).astype(half_type)
+        own_share = (own_expo / total).astype(half_type).astype(kind)
+        for item in range(batch):
+            seq = at * batch + item
+            part = slice(item * HEADS, (item + 1) * HEADS)
+            result = jnp.dot(share[part], values_s[seq], preferred_element_type=kind)
+            result = result + own_share[part] * value_s[pl.ds(seq, 1), :]
+            heads_s[pl.ds(pl.multiple_of(seq * HEADS, HEADS), HEADS), :] = result
+
+    for at in range(9, len(loads) + 6):
+        copies[at].wait()
+
+    found = [heads_s[pl.ds(head, seqs, stride=HEADS), :] for head in range(HEADS)]
+    pieces = []
+    for tile in range(tiles):
+        left, right = found[2 * tile], found[2 * tile + 1]
+        if 2 * tile // group:
+            left = pltpu.roll(left, HEAD_DIM, 1)
+        else:
+            right = pltpu.roll(right, HEAD_DIM, 1)
+        pieces.append(jnp.where(lane < HEAD_DIM, left, right))
+    attended = jnp.concatenate(pieces, axis=1).astype(half_type)
+    mixed = tokens_s[...].astype(kind) + jnp.dot(
+        attended, w_out_s[...], preferred_element_type=kind
+    )
+    mixed = mixed.astype(half_type).astype(kind)
+    mixed_s[...] = mixed
+    routed = normalize(mixed, gain_next_s[...])
+
+    def slot(at, which, place):
+        return (at * 2 + which) * plane + place
+
+    home = slot(level, core, spot)
+    for part in range(folds):
+        fold_s[pl.ds(part * spare, spare), :] = routed[block:, part * fold : (part + 1) * fold]
+    rows_s[home, :, 0:width] = routed[:block].astype(half_type)
+    rows_s[home, :, width:wide] = fold_s[...].astype(half_type)
+
+    experts = lax.broadcasted_iota(jnp.int32, (n, seqs), 0)
+    matched = jnp.zeros((n, seqs), kind)
+    for at in range(TOPK):
+        chosen = ids_s[at : at + 1, :] == experts
+        matched = matched + jnp.where(chosen, weights_s[at : at + 1, :], 0.0)
+    token = lax.broadcasted_iota(jnp.int32, (seqs, bulk), 0)
+    spread = lax.broadcasted_iota(jnp.int32, (seqs, bulk), 1)
+    member = core * plane + spot
+    exact = lax.Precision.HIGHEST
+
+    def placed(place):
+        return jnp.dot(
+            matched, jnp.where(place, 1.0, 0.0), preferred_element_type=kind, precision=exact
+        )
+
+    main_row = placed((token < block) & (spread == member * block + token))
+    tail_row = placed(
+        (token >= block) & (spread == level * tail + (token - block) * members + member)
+    )
+    line = lax.broadcasted_iota(jnp.int32, square_s.shape, 0)
+    for at in range(n):
+        info_s[at] = jnp.where(
+            line == level,
+            main_row[at : at + 1, :],
+            jnp.where(line == deep, tail_row[at : at + 1, :], 0.0),
+        )
+
+    def device(z, y, x, which):
+        return ((z * side + y) * side + x) * 2 + which
+
+    spot_x = row * side + 1 - col
+    spot_y = (1 - row) * side + col
+    spot_d = (1 - row) * side + 1 - col
+    near_x = device(level, row, 1 - col, core)
+    near_y = device(level, 1 - row, col, core)
+
+    def along(at, way):
+        place = rows_s.at[slot(at, core, spot)]
+        to = device(level + (1 if way else -1), row, col, core)
+        return reach(place, place, z_send.at[way, at], z_recv.at[at], to)
+
+    def beside(at, place):
+        here = rows_s.at[slot(at, core, place)]
+        return reach(here, here, x_send.at[at], x_recv.at[at], near_x)
+
+    def above(at, place):
+        here = rows_s.at[slot(at, core, place)]
+        return reach(here, here, y_send.at[at], y_recv.at[at], near_y)
+
+    def relay_a(at, place):
+        here = rows_s.at[slot(at, core, place), :, 0:cut]
+        return reach(here, here, da_send.at[at], da_recv.at[at], near_y)
+
+    def relay_b(at, place):
+        here = rows_s.at[slot(at, core, place), :, cut:wide]
+        return reach(here, here, db_send.at[at], db_recv.at[at], near_x)
+
+    def across(at, which, place):
+        here = rows_s.at[slot(at, which, place)]
+        return reach(here, here, f_send.at[at, place], f_recv.at[at, place], other)
+
+    balance = jnp.minimum(level, deep - 1 - level)
+    lean = jnp.where(2 * level < deep - 1, 1, -1)
+
+    def ordered(j):
+        paired = jnp.where(lax.rem(j, 2) == 1, -1, 1) * ((j + 1) // 2)
+        single = lean * (j - balance)
+        return level + jnp.where(j <= 2 * balance, paired, single)
+
+    def inform(k):
+        to = lax.rem(me + k, n)
+        return reach(info_s.at[to], infos_s.at[k], i_send.at[k], i_recv.at[k], to)
+
+    def informed(k):
+        return reach(info_s.at[0], infos_s.at[k], i_send.at[k], i_recv.at[k], lax.rem(me + k, n))
+
+    def share(k):
+        return reach(square_s, squares_s.at[k], q_send.at[k], q_recv.at[k], lax.rem(me + k, n))
+
+    pl.semaphore_wait(barrier, n - 1)
+
+    def spread_native(at):
+        beside(at, spot).start()
+        above(at, spot).start()
+        across(at, core, spot).start()
+
+    @pl.when(level + 1 < deep)
+    def _():
+        along(level, 1).start()
+
+    @pl.when(level > 0)
+    def _():
+        along(level, 0).start()
+
+    spread_native(level)
+
+    @pl.loop(1, n)
+    def _(k):
+        inform(k).start()
+
+    infos_s[0] = info_s[me]
+
+    for at in range(len(loads) + 6, len(loads) + len(later)):
+        copies[at].wait()
+
+    ones = jnp.ones((8, pair), kind)
+    same_bulk = lax.broadcasted_iota(jnp.int32, (bulk, bulk), 0)
+    same_bulk = same_bulk == lax.broadcasted_iota(jnp.int32, (bulk, bulk), 1)
+    tail_at = lax.broadcasted_iota(jnp.int32, (tail, bulk), 1)
+    tail_of = lax.broadcasted_iota(jnp.int32, (tail, bulk), 0)
+
+    square_s[...] = jnp.zeros_like(square_s)
+
+    @pl.loop(0, deep)
+    def _(j):
+        at = ordered(j)
+        beside(at, spot_x).wait_recv()
+        relay_a(at, spot_x).start()
+        across(at, core, spot_x).start()
+        above(at, spot_y).wait_recv()
+        relay_b(at, spot_y).start()
+        across(at, core, spot_y).start()
+
+        @pl.when(j + 1 < deep)
+        def _():
+            following = ordered(j + 1)
+            along(following, 0).wait_recv()
+
+            @pl.when((following < level) & (level + 1 < deep))
+            def _():
+                along(following, 1).start()
+
+            @pl.when((following > level) & (level > 0))
+            def _():
+                along(following, 0).start()
+
+            spread_native(following)
+
+        relay_a(at, spot_d).wait_recv()
+        relay_b(at, spot_d).wait_recv()
+        across(at, core, spot_d).start()
+        for place in range(plane):
+            across(at, 1 - core, place).wait_recv()
+
+        part = pl.ds(at * members, members)
+        x_s[at, 0:bulk, :] = rows_s[part, :, 0:width].reshape(bulk, width)
+        folded = rows_s[part, :, width:wide].astype(kind).reshape(bulk, fold)
+        for tile in range(fold // pair):
+            spread_s[tile] = folded[:, tile * pair : (tile + 1) * pair]
+        for piece in range(folds):
+            for tile in range(fold // pair):
+                lanes = slice(piece * fold + tile * pair, piece * fold + (tile + 1) * pair)
+                taken = [
+                    spread_s[tile, pl.ds(piece * spare + extra, members, stride=block), :]
+                    for extra in range(spare)
+                ]
+                x_s[at, bulk : bulk + tail, lanes] = jnp.concatenate(taken, axis=0).astype(
+                    half_type
+                )
+        values = x_s[at]
+        inner = jnp.sum(values.astype(kind) * branch_s[...], axis=1, keepdims=True)
+        branch_col_s[at] = jnp.broadcast_to(jax.nn.sigmoid(inner), (bulk + tail, pair))
+        both = jnp.dot(values, d_in_s[...], preferred_element_type=kind)
+        gate, up = both[:, 0:pair], both[:, pair : 2 * pair]
+        units = (gate * jax.nn.sigmoid(gate) * up).astype(half_type).astype(kind)
+        hidden_s[at] = (units * d_gain_s[pl.ds(me, 1), :]).astype(half_type)
+        squares = lax.dot_general(
+            ones,
+            units * units,
+            (((1,), (1,)), ((), ())),
+            preferred_element_type=kind,
+            precision=exact,
+        )
+        square_s[pl.ds(at, 1), :] = squares[0:1, 0:bulk]
+        ends = jnp.sum(units[bulk:] * units[bulk:], axis=1, keepdims=True)
+        ends = jnp.sum(jnp.where(tail_at == at * tail + tail_of, ends, 0.0), axis=0, keepdims=True)
+        square_s[deep : deep + 1, :] = square_s[deep : deep + 1, :] + ends
+
+        @pl.when(j + 1 == deep)
+        def _():
+            @pl.loop(1, n)
+            def _(k):
+                share(k).start()
+
+        gate = jnp.minimum(jnp.dot(values, e_gate_s[...], preferred_element_type=kind), LIMIT)
+        up = jnp.clip(jnp.dot(values, e_up_s[...], preferred_element_type=kind), -LIMIT, LIMIT)
+        act = ((up + 1.0) * gate * jax.nn.sigmoid(gate * ALPHA)).astype(half_type)
+        answer_s[at] = jnp.dot(act, e_down_s[...], preferred_element_type=kind).astype(half_type)
+
+    @pl.loop(1, n)
+    def _(k):
+        informed(k).wait_recv()
+        share(k).wait_recv()
+
+    coef_s[...] = jnp.sum(infos_s[...], axis=0)
+    squares_s[0] = square_s[...]
+    scale_s[...] = lax.rsqrt(jnp.sum(squares_s[...], axis=0) / units_total + EPS)
+
+    def columns(ref, at):
+        main = to_column(ref[pl.ds(at, 1), :], same_bulk)
+        ends = jnp.where(tail_at == at * tail + tail_of, ref[deep : deep + 1, :], 0.0)
+        return main, jnp.sum(ends, axis=1, keepdims=True)
+
+    def cross(at):
+        return reach(
+            part_s.at[at, pl.ds((1 - core) * plane, plane)],
+            joint_s.at[at],
+            c_send.at[at],
+            c_recv.at[at],
+            other,
+        )
+
+    def first(at, k):
+        return (
+            reach(
+                pair_s.at[at, k * side + 1 - col, :, 0:cut],
+                first_a.at[at, k],
+                s1a_send.at[at, k],
+                s1a_recv.at[at, k],
+                near_x,
+            ),
+            reach(
+                pair_s.at[at, (1 - row) * side + k, :, cut:wide],
+                first_b.at[at, k],
+                s1b_send.at[at, k],
+                s1b_recv.at[at, k],
+                near_y,
+            ),
+        )
+
+    def second(at):
+        return (
+            reach(turn_a.at[at], second_a.at[at], s2a_send.at[at], s2a_recv.at[at], near_y),
+            reach(turn_b.at[at], second_b.at[at], s2b_send.at[at], s2b_recv.at[at], near_x),
+        )
+
+    def home_to(at):
+        return reach(
+            level_s.at[at],
+            levels_s.at[level],
+            zz_send.at[at],
+            zz_recv.at[level],
+            device(at, row, col, core),
+        )
+
+    def home_from(at):
+        return reach(
+            level_s.at[at],
+            levels_s.at[at],
+            zz_send.at[at],
+            zz_recv.at[at],
+            device(at, row, col, core),
+        )
+
+    @pl.loop(0, deep + 3)
+    def _(step):
+        @pl.when(step < deep)
+        def _():
+            at = ordered(deep - 1 - step)
+            dense = jnp.dot(hidden_s[at], d_down_s[...], preferred_element_type=kind)
+            weight, weight_end = columns(coef_s, at)
+            scale, scale_end = columns(scale_s, at)
+            twice = branch_col_s[at, :, 0:1]
+            main = weight * answer_s[at, 0:bulk, :].astype(kind)
+            main = main + (scale * twice[0:bulk]) * dense[0:bulk]
+            ends = weight_end * answer_s[at, bulk : bulk + tail, :].astype(kind)
+            ends = ends + (scale_end * twice[bulk:]) * dense[bulk:]
+            part_s[at, :, :, 0:width] = main.astype(half_type).reshape(members, block, width)
+            for piece in range(folds):
+                for tile in range(fold // pair):
+                    first_lane = piece * fold + tile * pair
+                    for extra in range(spare):
+                        spread_s[tile, pl.ds(piece * spare + extra, members, stride=block), :] = (
+                            ends[
+                                extra * members : (extra + 1) * members,
+                                first_lane : first_lane + pair,
+                            ]
+                        )
+            for tile in range(fold // pair):
+                part_s[at, :, :, width + tile * pair : width + (tile + 1) * pair] = (
+                    spread_s[tile].astype(half_type).reshape(members, block, pair)
+                )
+            cross(at).start()
+
+        @pl.when((step >= 1) & (step < deep + 1))
+        def _():
+            at = ordered(deep - step)
+            cross(at).wait_recv()
+            mine = part_s[at, pl.ds(core * plane, plane)].astype(kind)
+            pair_s[at] = (mine + joint_s[at].astype(kind)).astype(half_type)
+            for k in range(side):
+                for copy in first(at, k):
+                    copy.start()
+
+        @pl.when((step >= 2) & (step < deep + 2))
+        def _():
+            at = ordered(deep + 1 - step)
+            for k in range(side):
+                for copy in first(at, k):
+                    copy.wait_recv()
+            turned = pair_s[at, spot_y, :, 0:cut].astype(kind) + first_a[at, 1 - row].astype(kind)
+            turn_a[at] = turned.astype(half_type)
+            turned = pair_s[at, spot_x, :, cut:wide].astype(kind) + first_b[at, 1 - col].astype(kind)
+            turn_b[at] = turned.astype(half_type)
+            for copy in second(at):
+                copy.start()
+
+        @pl.when(step >= 3)
+        def _():
+            at = ordered(deep + 2 - step)
+            for copy in second(at):
+                copy.wait_recv()
+            total = pair_s[at, spot, :, 0:cut].astype(kind) + first_a[at, row].astype(kind)
+            total = total + second_a[at].astype(kind)
+            level_s[at, :, 0:cut] = total.astype(half_type)
+            total = pair_s[at, spot, :, cut:wide].astype(kind) + first_b[at, col].astype(kind)
+            total = total + second_b[at].astype(kind)
+            level_s[at, :, cut:wide] = total.astype(half_type)
+
+            @pl.when(step < deep + 2)
+            def _():
+                home_to(at).start()
+
+    total = level_s[level].astype(kind)
+    for j in range(1, deep):
+        at = ordered(j)
+        home_from(at).wait_recv()
+        total = total + levels_s[at].astype(kind)
+    out[0:block, :] = (mixed_s[0:block, :] + total[:, 0:width]).astype(half_type)
+    fold_s[...] = total[:, width:wide]
+    for part in range(folds):
+        lanes = slice(part * fold, (part + 1) * fold)
+        ends = mixed_s[block:seqs, lanes] + fold_s[pl.ds(part * spare, spare), :]
+        out[block:seqs, lanes] = ends.astype(half_type)
+
+    @pl.loop(0, deep)
+    def _(at):
+        @pl.when((at <= level) & (level + 1 < deep))
+        def _():
+            along(at, 1).wait_send()
+
+        @pl.when((at >= level) & (level > 0))
+        def _():
+            along(at, 0).wait_send()
+
+        beside(at, spot).wait_send()
+        above(at, spot).wait_send()
+        relay_a(at, spot_x).wait_send()
+        relay_b(at, spot_y).wait_send()
+        for place in range(plane):
+            across(at, core, place).wait_send()
+        cross(at).wait_send()
+        for k in range(side):
+            for copy in first(at, k):
+                copy.wait_send()
+        for copy in second(at):
+            copy.wait_send()
+
+        @pl.when(at != level)
+        def _():
+            home_to(at).wait_send()
+
+    @pl.loop(1, n)
+    def _(k):
+        informed(k).wait_send()
+        share(k).wait_send()
+
+
+def fast(n, deep, arrays, units_total):
+    (tokens, keys, logcum, e_gate, e_down, d_gate, d_gain) = (
+        arrays[0],
+        arrays[8],
+        arrays[10],
+        arrays[15],
+        arrays[17],
+        arrays[18],
+        arrays[21],
+    )
+    seqs, width = tokens.shape
+    length, pair = keys.shape[1:]
+    hidden = e_gate.shape[2]
+    local = d_gate.shape[1]
+    chips = n // 2
+    plane = chips // deep
+    block = seqs // 16 * 16
+    spare = seqs - block
+    wide = width + spare * width // block
+    fold = wide - width
+    cut = wide // 2
+    members = 2 * plane
+    bulk = members * block
+    tail = members * spare
+    heads_wide = HEADS * HEAD_DIM
+    half_type = jnp.bfloat16
+    kind = jnp.float32
+    dma = pltpu.SemaphoreType.DMA
+    groups = 6
+    vmem = pltpu.VMEM
+    scratch = [
+        vmem((seqs, width), half_type),
+        vmem((1, width), kind),
+        vmem((width, heads_wide + 2 * pair), half_type),
+        vmem((HEADS, width), half_type),
+        vmem((1, HEADS), kind),
+        vmem((heads_wide, width), half_type),
+        vmem((seqs, length, pair), half_type),
+        vmem((seqs, length, pair), half_type),
+        vmem((seqs, HEADS, length), kind),
+        pltpu.SMEM((seqs,), jnp.int32),
+        vmem((1, width), kind),
+        vmem((TOPK, seqs), jnp.int32),
+        vmem((TOPK, seqs), kind),
+        vmem((width, hidden), half_type),
+        vmem((width, hidden), half_type),
+        vmem((hidden, width), half_type),
+        vmem((width, 2 * local), half_type),
+        vmem((local, width), half_type),
+        vmem(d_gain.shape, kind),
+        vmem((1, width), kind),
+        vmem((seqs * HEADS, pair), kind),
+        vmem((seqs, pair), kind),
+        vmem((seqs, pair), kind),
+        vmem((HEADS, seqs), kind),
+        vmem((8, pair), kind),
+        vmem((seqs * HEADS, pair), kind),
+        vmem((seqs, width), kind),
+        vmem((block, fold), kind),
+        vmem((n, block, wide), half_type),
+        vmem((deep, bulk + tail, width), half_type),
+        vmem((fold // pair, bulk, pair), kind),
+        vmem((deep, bulk + tail, local), half_type),
+        vmem((deep, bulk + tail, pair), kind),
+        vmem((8, bulk), kind),
+        vmem((n, 8, bulk), kind),
+        vmem((n, 8, bulk), kind),
+        vmem((n, 8, bulk), kind),
+        vmem((8, bulk), kind),
+        vmem((8, bulk), kind),
+        vmem((deep, bulk + tail, width), half_type),
+        vmem((deep, members, block, wide), half_type),
+        vmem((deep, plane, block, wide), half_type),
+        vmem((deep, plane, block, wide), half_type),
+        vmem((deep, 2, block, cut), half_type),
+        vmem((deep, 2, block, cut), half_type),
+        vmem((deep, block, cut), half_type),
+        vmem((deep, block, cut), half_type),
+        vmem((deep, block, cut), half_type),
+        vmem((deep, block, cut), half_type),
+        vmem((deep, block, wide), half_type),
+        vmem((deep, block, wide), half_type),
+        dma((21,)),
+        dma((2, groups)),
+        dma((2, deep)),
+        dma((deep,)),
+        dma((deep,)),
+        dma((deep,)),
+        dma((deep,)),
+        dma((deep,)),
+        dma((deep,)),
+        dma((deep,)),
+        dma((deep,)),
+        dma((deep,)),
+        dma((deep, plane)),
+        dma((deep, plane)),
+        dma((n,)),
+        dma((n,)),
+        dma((n,)),
+        dma((n,)),
+        dma((deep,)),
+        dma((deep,)),
+        dma((deep, 2)),
+        dma((deep, 2)),
+        dma((deep, 2)),
+        dma((deep, 2)),
+        dma((deep,)),
+        dma((deep,)),
+        dma((deep,)),
+        dma((deep,)),
+        dma((deep,)),
+        dma((deep,)),
+    ]
+    return pl.pallas_call(
+        functools.partial(fast_body, units_total),
+        out_shape=jax.ShapeDtypeStruct(tokens.shape, half_type),
+        in_specs=[pl.BlockSpec(memory_space=pl.ANY)] * len(arrays),
+        out_specs=pl.BlockSpec(memory_space=pltpu.VMEM),
+        scratch_shapes=scratch,
+        compiler_params=pltpu.CompilerParams(
+            collective_id=0, has_side_effects=True, vmem_limit_bytes=62 * 1024 * 1024
+        ),
+        name="layer",
+    )(*arrays)
+
+
 def shards(
     tokens,
     attn_norm_gain,
@@ -557,6 +1343,43 @@
     dense_norm_gain,
     branch_gate,
 ):
+    n = lax.axis_size("ep")
+    deep = 4
+    seqs, width = tokens.shape
+    local = w_dense_gate.shape[1]
+    spare = seqs % 16
+    fits = n == 8 * deep and local == cache_keys.shape[2] and 0 < spare and spare * width % 2048 == 0
+    if fits and seqs // 16 == 1:
+        return fast(
+            n,
+            deep,
+            (
+                tokens,
+                attn_norm_gain[None, :],
+                w_query,
+                w_key,
+                w_value,
+                w_forget.T,
+                forget_bias[None, :],
+                w_attn_out,
+                cache_keys,
+                cache_values,
+                cache_logcum,
+                cache_lengths,
+                expert_norm_gain[None, :],
+                expert_ids.T,
+                expert_weights.T,
+                w_expert_gate,
+                w_expert_up,
+                w_expert_down,
+                w_dense_gate,
+                w_dense_up,
+                w_dense_down,
+                dense_norm_gain.reshape(n, local),
+                branch_gate[None, :],
+            ),
+            dense_norm_gain.shape[0],
+        )
     mixed, routed_in = front(
         tokens,
         attn_norm_gain,

time: 100 us -> 66.4 us (0.66)
  Pallas kernels: 80.5 us -> 64.7 us
  local copies, waits for them, and re-layouts: 16.9 us -> 1.54 us
  other arithmetic: 2.14 us -> 0 us
    pallas_call x2 -> x1, Pallas kernels: 80.5 us -> 64.7 us  [fast(): pl.pallas_call(functools.partial(fast_body, units_total), out_shape=jax.S...]
    unnamed x28 -> x1, local copies, waits for them, and re-layouts: 15.3 us -> 1.54 us
    convert_element_type x4 -> x0, other arithmetic: 1.41 us -> none  [the longest x3 0.72 us: stored(): return lax.optimization_barrier(values.astype(jnp.bfloat16))]
    broadcast_in_dim x2 -> x0, local copies, waits for them, and re-layouts: 1.32 us -> none  [the longest x1 0.73 us: front(): bias[:, None]]
where the time goes in v1:
time: 66.4 us; the launch traced here: 66.3 us
  Pallas kernels  64.7 us (97%)
  local copies, waits for them, and re-layouts  1.54 us (2%)
    pallas_call x1, Pallas kernels, fast(): pl.pallas_call(functools.partial(fast_body, units_total), out_shape=jax.S...  64.7 us
    unnamed x1, local copies, waits for them, and re-layouts  1.54 us

profile of v1, /device:TPU:0, one launch (start us, length us, event | category | flops | bytes accessed | tf_op | source)
XLA Modules:
  0.0 66.3 jit_solution(8070212872838091408)
XLA Ops:
  0.0 64.7 %layer.1 = bf16[18,2048]{1,0:T(8,128)(2,1)} custom-call(bf16[18,2048]{1,0:T(8,128)(2,1)} %tokens_h.1, f32[1,2048]{1,0:T(1,128)} %bitcast.10, bf16[2048,512]{1,0:T(8,128)(2,1)} %w_query_h.1, bf16[2048,128]{1,0:T(8,128)(2,1)} %w_key_h.1, bf16[2048,128]{1,0:T(8,128)(2,1)} %w_value_h.1, bf16[8,2048]{1,0:T(8,128)(2,1)} %bitcast.8, f32[1,8]{1,0:T(1,128)} %bitcast.15, ...), custom_call_target="tpu_custom_call" | custom-call | tf_op jit(solution)/shard_map/layer/pallas_call | solution.py:1308
  64.8 1.5 %copy.25 = bf16[18,2048]{1,0:T(8,128)(2,1)} copy(bf16[18,2048]{1,0:T(8,128)(2,1)} %layer.1) | data formatting | bytes 147456

commit v2 on v1

--- a/solution.py
+++ b/solution.py
@@ -582,7 +582,6 @@
     key_s,
     value_s,
     forget_s,
-    own_s,
     heads_s,
     mixed_s,
     fold_s,
@@ -596,7 +595,6 @@
     info_s,
     infos_s,
     scale_s,
-    coef_s,
     answer_s,
     part_s,
     joint_s,
@@ -613,31 +611,22 @@
     kv_sem,
     z_send,
     z_recv,
-    x_send,
+    rows_send,
     x_recv,
-    y_send,
     y_recv,
-    da_send,
     da_recv,
-    db_send,
     db_recv,
-    f_send,
     f_recv,
     i_send,
     i_recv,
     q_send,
     q_recv,
-    c_send,
+    back_send,
     c_recv,
-    s1a_send,
     s1a_recv,
-    s1b_send,
     s1b_recv,
-    s2a_send,
     s2a_recv,
-    s2b_send,
     s2b_recv,
-    zz_send,
     zz_recv,
 ):
     kind = jnp.float32
@@ -730,6 +719,27 @@
     for copy in copies[len(loads) :]:
         copy.start()
 
+    for at in (1, 2):
+        copies[len(loads) - at].wait()
+
+    experts = lax.broadcasted_iota(jnp.int32, (n, seqs), 0)
+    matched = jnp.zeros((n, seqs), kind)
+    for at in range(TOPK):
+        chosen = ids_s[at : at + 1, :] == experts
+        matched = matched + jnp.where(chosen, weights_s[at : at + 1, :], 0.0)
+    token = lax.broadcasted_iota(jnp.int32, (seqs, 2 * bulk), 0)
+    spread = lax.broadcasted_iota(jnp.int32, (seqs, 2 * bulk), 1)
+    member = core * plane + spot
+    exact = lax.Precision.HIGHEST
+    in_block = (token < block) & (spread == member * block + token)
+    in_tail = (token >= block) & (spread == bulk + (token - block) * members + member)
+    spread = jnp.where(in_block | in_tail, 1.0, 0.0)
+    spread = jnp.dot(matched, spread, preferred_element_type=kind, precision=exact)
+    for at in range(n):
+        info_s[at] = spread[at : at + 1, :]
+    infos_s[pl.ds(me, 1)] = info_s[pl.ds(me, 1)]
+    square_s[...] = jnp.zeros_like(square_s)
+
     for at in range(9):
         copies[at].wait()
 
@@ -757,8 +767,7 @@
     position = lax.broadcasted_iota(jnp.int32, (HEADS, length), 1)
     unit = HEAD_DIM ** (-0.5)
 
-    @pl.loop(0, groups)
-    def _(at):
+    def attend(at):
         for copy in cached(at):
             copy.wait()
         scores_all = []
@@ -795,7 +804,24 @@
             result = result + own_share[part] * value_s[pl.ds(seq, 1), :]
             heads_s[pl.ds(pl.multiple_of(seq * HEADS, HEADS), HEADS), :] = result
 
-    for at in range(9, len(loads) + 6):
+    def inform(k):
+        to = lax.rem(me + k, n)
+        return reach(info_s.at[to], infos_s.at[me], i_send.at[0], i_recv.at[0], to)
+
+    def informed():
+        every = infos_s.at[pl.ds(0, n - 1)]
+        return reach(every, every, i_send.at[0], i_recv.at[0], other)
+
+    pl.loop(0, groups // 2)(attend)
+    pl.semaphore_wait(barrier, n - 1)
+
+    @pl.loop(1, n)
+    def _(k):
+        inform(k).start()
+
+    pl.loop(groups // 2, groups)(attend)
+
+    for at in range(len(loads), len(loads) + 6):
         copies[at].wait()
 
     found = [heads_s[pl.ds(head, seqs, stride=HEADS), :] for head in range(HEADS)]
@@ -824,33 +850,6 @@
     rows_s[home, :, 0:width] = routed[:block].astype(half_type)
     rows_s[home, :, width:wide] = fold_s[...].astype(half_type)
 
-    experts = lax.broadcasted_iota(jnp.int32, (n, seqs), 0)
-    matched = jnp.zeros((n, seqs), kind)
-    for at in range(TOPK):
-        chosen = ids_s[at : at + 1, :] == experts
-        matched = matched + jnp.where(chosen, weights_s[at : at + 1, :], 0.0)
-    token = lax.broadcasted_iota(jnp.int32, (seqs, bulk), 0)
-    spread = lax.broadcasted_iota(jnp.int32, (seqs, bulk), 1)
-    member = core * plane + spot
-    exact = lax.Precision.HIGHEST
-
-    def placed(place):
-        return jnp.dot(
-            matched, jnp.where(place, 1.0, 0.0), preferred_element_type=kind, precision=exact
-        )
-
-    main_row = placed((token < block) & (spread == member * block + token))
-    tail_row = placed(
-        (token >= block) & (spread == level * tail + (token - block) * members + member)
-    )
-    line = lax.broadcasted_iota(jnp.int32, square_s.shape, 0)
-    for at in range(n):
-        info_s[at] = jnp.where(
-            line == level,
-            main_row[at : at + 1, :],
-            jnp.where(line == deep, tail_row[at : at + 1, :], 0.0),
-        )
-
     def device(z, y, x, which):
         return ((z * side + y) * side + x) * 2 + which
 
@@ -860,30 +859,37 @@
     near_x = device(level, row, 1 - col, core)
     near_y = device(level, 1 - row, col, core)
 
-    def along(at, way):
-        place = rows_s.at[slot(at, core, spot)]
+    def part_of(at, place, piece):
+        return rows_s.at[slot(at, core, place), :, piece * cut : (piece + 1) * cut]
+
+    def along(at, way, piece):
+        here = part_of(at, spot, piece)
         to = device(level + (1 if way else -1), row, col, core)
-        return reach(place, place, z_send.at[way, at], z_recv.at[at], to)
-
-    def beside(at, place):
-        here = rows_s.at[slot(at, core, place)]
-        return reach(here, here, x_send.at[at], x_recv.at[at], near_x)
-
-    def above(at, place):
-        here = rows_s.at[slot(at, core, place)]
-        return reach(here, here, y_send.at[at], y_recv.at[at], near_y)
+        return reach(here, here, z_send.at[way, at], z_recv.at[piece, at], to)
+
+    def beside(at, place, piece):
+        here = part_of(at, place, piece)
+        return reach(here, here, rows_send.at[0], x_recv.at[piece, at], near_x)
+
+    def above(at, place, piece):
+        here = part_of(at, place, piece)
+        return reach(here, here, rows_send.at[0], y_recv.at[piece, at], near_y)
 
     def relay_a(at, place):
         here = rows_s.at[slot(at, core, place), :, 0:cut]
-        return reach(here, here, da_send.at[at], da_recv.at[at], near_y)
+        return reach(here, here, rows_send.at[0], da_recv.at[at], near_y)
 
     def relay_b(at, place):
         here = rows_s.at[slot(at, core, place), :, cut:wide]
-        return reach(here, here, db_send.at[at], db_recv.at[at], near_x)
+        return reach(here, here, rows_send.at[0], db_recv.at[at], near_x)
 
     def across(at, which, place):
         here = rows_s.at[slot(at, which, place)]
-        return reach(here, here, f_send.at[at, place], f_recv.at[at, place], other)
+        return reach(here, here, rows_send.at[0], f_recv.at[at], other)
+
+    def crossed(at):
+        here = rows_s.at[pl.ds(slot(at, 1 - core, 0), plane)]
+        return reach(here, here, rows_send.at[0], f_recv.at[at], other)
 
     balance = jnp.minimum(level, deep - 1 - level)
     lean = jnp.where(2 * level < deep - 1, 1, -1)
@@ -893,38 +899,44 @@
         single = lean * (j - balance)
         return level + jnp.where(j <= 2 * balance, paired, single)
 
-    def inform(k):
-        to = lax.rem(me + k, n)
-        return reach(info_s.at[to], infos_s.at[k], i_send.at[k], i_recv.at[k], to)
-
-    def informed(k):
-        return reach(info_s.at[0], infos_s.at[k], i_send.at[k], i_recv.at[k], lax.rem(me + k, n))
-
-    def share(k):
-        return reach(square_s, squares_s.at[k], q_send.at[k], q_recv.at[k], lax.rem(me + k, n))
-
-    pl.semaphore_wait(barrier, n - 1)
-
-    def spread_native(at):
-        beside(at, spot).start()
-        above(at, spot).start()
-        across(at, core, spot).start()
-
-    @pl.when(level + 1 < deep)
-    def _():
-        along(level, 1).start()
-
-    @pl.when(level > 0)
-    def _():
-        along(level, 0).start()
-
-    spread_native(level)
-
-    @pl.loop(1, n)
-    def _(k):
-        inform(k).start()
-
-    infos_s[0] = info_s[me]
+    def share(k, at):
+        return reach(
+            square_s.at[at],
+            squares_s.at[k, at],
+            q_send.at[0],
+            q_recv.at[0],
+            lax.rem(me + k, n),
+        )
+
+    def shared():
+        every = squares_s.at[pl.ds(1, n - 1)]
+        return reach(every, every, q_send.at[0], q_recv.at[0], other)
+
+    def sent(blocks, sem):
+        every = rows_s.at[pl.ds(0, blocks)]
+        return reach(every, every, sem, sem, other)
+
+    def spread_piece(at, piece):
+        if piece:
+            above(at, spot, piece).start()
+            beside(at, spot, piece).start()
+        else:
+            beside(at, spot, piece).start()
+            above(at, spot, piece).start()
+
+    for piece in range(2):
+
+        @pl.when(level + 1 < deep)
+        def _():
+            along(level, 1, piece).start()
+
+        @pl.when(level > 0)
+        def _():
+            along(level, 0, piece).start()
+
+        spread_piece(level, piece)
+
+    across(level, core, spot).start()
 
     for at in range(len(loads) + 6, len(loads) + len(later)):
         copies[at].wait()
@@ -935,38 +947,8 @@
     tail_at = lax.broadcasted_iota(jnp.int32, (tail, bulk), 1)
     tail_of = lax.broadcasted_iota(jnp.int32, (tail, bulk), 0)
 
-    square_s[...] = jnp.zeros_like(square_s)
-
-    @pl.loop(0, deep)
-    def _(j):
-        at = ordered(j)
-        beside(at, spot_x).wait_recv()
-        relay_a(at, spot_x).start()
-        across(at, core, spot_x).start()
-        above(at, spot_y).wait_recv()
-        relay_b(at, spot_y).start()
-        across(at, core, spot_y).start()
-
-        @pl.when(j + 1 < deep)
-        def _():
-            following = ordered(j + 1)
-            along(following, 0).wait_recv()
-
-            @pl.when((following < level) & (level + 1 < deep))
-            def _():
-                along(following, 1).start()
-
-            @pl.when((following > level) & (level > 0))
-            def _():
-                along(following, 0).start()
-
-            spread_native(following)
-
-        relay_a(at, spot_d).wait_recv()
-        relay_b(at, spot_d).wait_recv()
-        across(at, core, spot_d).start()
-        for place in range(plane):
-            across(at, 1 - core, place).wait_recv()
+    def dense_units(at):
+        crossed(at).wait_recv()
 
         part = pl.ds(at * members, members)
         x_s[at, 0:bulk, :] = rows_s[part, :, 0:width].reshape(bulk, width)
@@ -997,41 +979,86 @@
             preferred_element_type=kind,
             precision=exact,
         )
-        square_s[pl.ds(at, 1), :] = squares[0:1, 0:bulk]
-        ends = jnp.sum(units[bulk:] * units[bulk:], axis=1, keepdims=True)
-        ends = jnp.sum(jnp.where(tail_at == at * tail + tail_of, ends, 0.0), axis=0, keepdims=True)
-        square_s[deep : deep + 1, :] = square_s[deep : deep + 1, :] + ends
-
-        @pl.when(j + 1 == deep)
-        def _():
-            @pl.loop(1, n)
-            def _(k):
-                share(k).start()
-
+        square_s[at, :, 0:bulk] = squares[0:1, 0:bulk]
+        square_s[at, :, bulk : bulk + tail] = squares[0:1, bulk : bulk + tail]
+
+        @pl.loop(1, n)
+        def _(k):
+            share(k, at).start()
+
+    def run_expert(at):
+        values = x_s[at]
         gate = jnp.minimum(jnp.dot(values, e_gate_s[...], preferred_element_type=kind), LIMIT)
         up = jnp.clip(jnp.dot(values, e_up_s[...], preferred_element_type=kind), -LIMIT, LIMIT)
         act = ((up + 1.0) * gate * jax.nn.sigmoid(gate * ALPHA)).astype(half_type)
         answer_s[at] = jnp.dot(act, e_down_s[...], preferred_element_type=kind).astype(half_type)
 
-    @pl.loop(1, n)
-    def _(k):
-        informed(k).wait_recv()
-        share(k).wait_recv()
-
-    coef_s[...] = jnp.sum(infos_s[...], axis=0)
+    @pl.loop(0, deep + 1)
+    def _(step):
+        @pl.when(step + 1 < deep)
+        def _():
+            at = ordered(step + 1)
+            for piece in range(2):
+                along(at, 0, piece).wait_recv()
+
+                @pl.when((at < level) & (level + 1 < deep))
+                def _():
+                    along(at, 1, piece).start()
+
+                @pl.when((at > level) & (level > 0))
+                def _():
+                    along(at, 0, piece).start()
+
+                spread_piece(at, piece)
+            across(at, core, spot).start()
+
+        @pl.when(step < deep)
+        def _():
+            at = ordered(step)
+            beside(at, spot_x, 0).wait_recv()
+            relay_a(at, spot_x).start()
+            above(at, spot_y, 1).wait_recv()
+            relay_b(at, spot_y).start()
+            beside(at, spot_x, 1).wait_recv()
+            across(at, core, spot_x).start()
+            above(at, spot_y, 0).wait_recv()
+            across(at, core, spot_y).start()
+
+        @pl.when(step >= 1)
+        def _():
+            at = ordered(step - 1)
+            relay_a(at, spot_d).wait_recv()
+            relay_b(at, spot_d).wait_recv()
+            across(at, core, spot_d).start()
+
+        @pl.when((step >= 2) & (step < deep))
+        def _():
+            run_expert(ordered(step - 2))
+
+        @pl.when(step >= 1)
+        def _():
+            dense_units(ordered(step - 1))
+
+    @pl.loop(deep - 2, deep)
+    def _(step):
+        run_expert(ordered(step))
+
+    informed().wait_recv()
+    shared().wait_recv()
+
     squares_s[0] = square_s[...]
     scale_s[...] = lax.rsqrt(jnp.sum(squares_s[...], axis=0) / units_total + EPS)
 
-    def columns(ref, at):
-        main = to_column(ref[pl.ds(at, 1), :], same_bulk)
-        ends = jnp.where(tail_at == at * tail + tail_of, ref[deep : deep + 1, :], 0.0)
+    def columns(line):
+        main = to_column(line[:, 0:bulk], same_bulk)
+        ends = jnp.where(tail_at == tail_of, line[:, bulk : 2 * bulk], 0.0)
         return main, jnp.sum(ends, axis=1, keepdims=True)
 
     def cross(at):
         return reach(
             part_s.at[at, pl.ds((1 - core) * plane, plane)],
             joint_s.at[at],
-            c_send.at[at],
+            back_send.at[0],
             c_recv.at[at],
             other,
         )
@@ -1041,30 +1068,30 @@
             reach(
                 pair_s.at[at, k * side + 1 - col, :, 0:cut],
                 first_a.at[at, k],
-                s1a_send.at[at, k],
-                s1a_recv.at[at, k],
+                back_send.at[0],
+                s1a_recv.at[at],
                 near_x,
             ),
             reach(
                 pair_s.at[at, (1 - row) * side + k, :, cut:wide],
                 first_b.at[at, k],
-                s1b_send.at[at, k],
-                s1b_recv.at[at, k],
+                back_send.at[0],
+                s1b_recv.at[at],
                 near_y,
             ),
         )
 
     def second(at):
         return (
-            reach(turn_a.at[at], second_a.at[at], s2a_send.at[at], s2a_recv.at[at], near_y),
-            reach(turn_b.at[at], second_b.at[at], s2b_send.at[at], s2b_recv.at[at], near_x),
+            reach(turn_a.at[at], second_a.at[at], back_send.at[0], s2a_recv.at[at], near_y),
+            reach(turn_b.at[at], second_b.at[at], back_send.at[0], s2b_recv.at[at], near_x),
         )
 
     def home_to(at):
         return reach(
             level_s.at[at],
             levels_s.at[level],
-            zz_send.at[at],
+            back_send.at[0],
             zz_recv.at[level],
             device(at, row, col, core),
         )
@@ -1073,7 +1100,7 @@
         return reach(
             level_s.at[at],
             levels_s.at[at],
-            zz_send.at[at],
+            back_send.at[0],
             zz_recv.at[at],
             device(at, row, col, core),
         )
@@ -1084,8 +1111,9 @@
         def _():
             at = ordered(deep - 1 - step)
             dense = jnp.dot(hidden_s[at], d_down_s[...], preferred_element_type=kind)
-            weight, weight_end = columns(coef_s, at)
-            scale, scale_end = columns(scale_s, at)
+            coef = jnp.sum(infos_s[pl.ds(at * members, members)], axis=0)
+            weight, weight_end = columns(coef)
+            scale, scale_end = columns(scale_s[at])
             twice = branch_col_s[at, :, 0:1]
             main = weight * answer_s[at, 0:bulk, :].astype(kind)
             main = main + (scale * twice[0:bulk]) * dense[0:bulk]
@@ -1121,9 +1149,8 @@
         @pl.when((step >= 2) & (step < deep + 2))
         def _():
             at = ordered(deep + 1 - step)
-            for k in range(side):
-                for copy in first(at, k):
-                    copy.wait_recv()
+            for here, sem in ((first_a.at[at], s1a_recv.at[at]), (first_b.at[at], s1b_recv.at[at])):
+                reach(here, here, back_send.at[0], sem, other).wait_recv()
             turned = pair_s[at, spot_y, :, 0:cut].astype(kind) + first_a[at, 1 - row].astype(kind)
             turn_a[at] = turned.astype(half_type)
             turned = pair_s[at, spot_x, :, cut:wide].astype(kind) + first_b[at, 1 - col].astype(kind)
@@ -1161,35 +1188,20 @@
 
     @pl.loop(0, deep)
     def _(at):
+        whole = rows_s.at[slot(at, core, spot)]
+
         @pl.when((at <= level) & (level + 1 < deep))
         def _():
-            along(at, 1).wait_send()
+            reach(whole, whole, z_send.at[1, at], z_send.at[1, at], other).wait_send()
 
         @pl.when((at >= level) & (level > 0))
         def _():
-            along(at, 0).wait_send()
-
-        beside(at, spot).wait_send()
-        above(at, spot).wait_send()
-        relay_a(at, spot_x).wait_send()
-        relay_b(at, spot_y).wait_send()
-        for place in range(plane):
-            across(at, core, place).wait_send()
-        cross(at).wait_send()
-        for k in range(side):
-            for copy in first(at, k):
-                copy.wait_send()
-        for copy in second(at):
-            copy.wait_send()
-
-        @pl.when(at != level)
-        def _():
-            home_to(at).wait_send()
-
-    @pl.loop(1, n)
-    def _(k):
-        informed(k).wait_send()
-        share(k).wait_send()
+            reach(whole, whole, z_send.at[0, at], z_send.at[0, at], other).wait_send()
+
+    sent(chips + 3 * deep, rows_send.at[0]).wait_send()
+    sent(chips + 4 * deep - 1, back_send.at[0]).wait_send()
+    informed().wait_send()
+    shared().wait_send()
 
 
 def fast(n, deep, arrays, units_total):
@@ -1220,7 +1232,7 @@
     half_type = jnp.bfloat16
     kind = jnp.float32
     dma = pltpu.SemaphoreType.DMA
-    groups = 6
+    groups = 3
     vmem = pltpu.VMEM
     scratch = [
         vmem((seqs, width), half_type),
@@ -1247,7 +1259,6 @@
         vmem((seqs, pair), kind),
         vmem((seqs, pair), kind),
         vmem((HEADS, seqs), kind),
-        vmem((8, pair), kind),
         vmem((seqs * HEADS, pair), kind),
         vmem((seqs, width), kind),
         vmem((block, fold), kind),
@@ -1256,12 +1267,11 @@
         vmem((fold // pair, bulk, pair), kind),
         vmem((deep, bulk + tail, local), half_type),
         vmem((deep, bulk + tail, pair), kind),
-        vmem((8, bulk), kind),
-        vmem((n, 8, bulk), kind),
-        vmem((n, 8, bulk), kind),
-        vmem((n, 8, bulk), kind),
-        vmem((8, bulk), kind),
-        vmem((8, bulk), kind),
+        vmem((deep, 1, 2 * bulk), kind),
+        vmem((n, deep, 1, 2 * bulk), kind),
+        vmem((n, 1, 2 * bulk), kind),
+        vmem((n, 1, 2 * bulk), kind),
+        vmem((deep, 1, 2 * bulk), kind),
         vmem((deep, bulk + tail, width), half_type),
         vmem((deep, members, block, wide), half_type),
         vmem((deep, plane, block, wide), half_type),
@@ -1277,27 +1287,18 @@
         dma((21,)),
         dma((2, groups)),
         dma((2, deep)),
+        dma((2, deep)),
+        dma((1,)),
+        dma((2, deep)),
+        dma((2, deep)),
         dma((deep,)),
         dma((deep,)),
         dma((deep,)),
-        dma((deep,)),
-        dma((deep,)),
-        dma((deep,)),
-        dma((deep,)),
-        dma((deep,)),
-        dma((deep,)),
-        dma((deep, plane)),
-        dma((deep, plane)),
-        dma((n,)),
-        dma((n,)),
-        dma((n,)),
-        dma((n,)),
-        dma((deep,)),
-        dma((deep,)),
-        dma((deep, 2)),
-        dma((deep, 2)),
-        dma((deep, 2)),
-        dma((deep, 2)),
+        dma((1,)),
+        dma((1,)),
+        dma((1,)),
+        dma((1,)),
+        dma((1,)),
         dma((deep,)),
         dma((deep,)),
         dma((deep,)),

time: 66.4 us -> 56.3 us (0.85)
  Pallas kernels: 64.7 us -> 54.6 us
    pallas_call x1, Pallas kernels: 64.7 us -> 54.6 us  [fast(): pl.pallas_call(functools.partial(fast_body, units_total), out_shape=jax.S...]
where the time goes in v2:
time: 56.3 us; the launch traced here: 56.1 us
  Pallas kernels  54.6 us (97%)
  local copies, waits for them, and re-layouts  1.54 us (3%)
    pallas_call x1, Pallas kernels, fast(): pl.pallas_call(functools.partial(fast_body, units_total), out_shape=jax.S...  54.6 us
    unnamed x1, local copies, waits for them, and re-layouts  1.54 us

profile of v2, /device:TPU:0, one launch (start us, length us, event | category | flops | bytes accessed | tf_op | source)
XLA Modules:
  0.0 56.1 jit_solution(10992823252667524360)
XLA Ops:
  0.0 54.6 %layer.1 = bf16[18,2048]{1,0:T(8,128)(2,1)} custom-call(bf16[18,2048]{1,0:T(8,128)(2,1)} %tokens_h.1, f32[1,2048]{1,0:T(1,128)} %bitcast.10, bf16[2048,512]{1,0:T(8,128)(2,1)} %w_query_h.1, bf16[2048,128]{1,0:T(8,128)(2,1)} %w_key_h.1, bf16[2048,128]{1,0:T(8,128)(2,1)} %w_value_h.1, bf16[8,2048]{1,0:T(8,128)(2,1)} %bitcast.8, f32[1,8]{1,0:T(1,128)} %bitcast.15, ...), custom_call_target="tpu_custom_call" | custom-call | tf_op jit(solution)/shard_map/layer/pallas_call | solution.py:1309
  54.6 1.5 %copy.25 = bf16[18,2048]{1,0:T(8,128)(2,1)} copy(bf16[18,2048]{1,0:T(8,128)(2,1)} %layer.1) | data formatting | bytes 147456

commit v3 on v2

--- a/solution.py
+++ b/solution.py
@@ -594,7 +594,6 @@
     squares_s,
     info_s,
     infos_s,
-    scale_s,
     answer_s,
     part_s,
     joint_s,
@@ -609,7 +608,6 @@
     levels_s,
     ld,
     kv_sem,
-    z_send,
     z_recv,
     rows_send,
     x_recv,
@@ -631,7 +629,7 @@
 ):
     kind = jnp.float32
     half_type = jnp.bfloat16
-    n = squares_s.shape[0]
+    n = infos_s.shape[0]
     chips = n // 2
     deep = x_s.shape[0]
     plane = chips // deep
@@ -862,10 +860,10 @@
     def part_of(at, place, piece):
         return rows_s.at[slot(at, core, place), :, piece * cut : (piece + 1) * cut]
 
-    def along(at, way, piece):
+    def along(at, to, piece):
         here = part_of(at, spot, piece)
-        to = device(level + (1 if way else -1), row, col, core)
-        return reach(here, here, z_send.at[way, at], z_recv.at[piece, at], to)
+        to = device(to, row, col, core)
+        return reach(here, here, rows_send.at[0], z_recv.at[piece, at], to)
 
     def beside(at, place, piece):
         here = part_of(at, place, piece)
@@ -899,18 +897,25 @@
         single = lean * (j - balance)
         return level + jnp.where(j <= 2 * balance, paired, single)
 
+    rank = jnp.where(level == 0, deep - 2, jnp.where(level == deep - 1, level, level - 1))
+
+    def returned(j):
+        k = j + jnp.where(j >= rank, 1, 0)
+        k = jnp.where(k < deep - 2, k + 1, jnp.where(k == deep - 2, 0, deep - 1))
+        return jnp.where(j == deep - 1, level, k)
+
     def share(k, at):
         return reach(
             square_s.at[at],
-            squares_s.at[k, at],
+            squares_s.at[at, k],
             q_send.at[0],
-            q_recv.at[0],
+            q_recv.at[at],
             lax.rem(me + k, n),
         )
 
-    def shared():
-        every = squares_s.at[pl.ds(1, n - 1)]
-        return reach(every, every, q_send.at[0], q_recv.at[0], other)
+    def shared(at):
+        every = squares_s.at[at, pl.ds(1, n - 1)]
+        return reach(every, every, q_send.at[0], q_recv.at[at], other)
 
     def sent(blocks, sem):
         every = rows_s.at[pl.ds(0, blocks)]
@@ -925,16 +930,12 @@
             above(at, spot, piece).start()
 
     for piece in range(2):
-
-        @pl.when(level + 1 < deep)
-        def _():
-            along(level, 1, piece).start()
-
-        @pl.when(level > 0)
-        def _():
-            along(level, 0, piece).start()
-
         spread_piece(level, piece)
+
+    @pl.loop(1, deep)
+    def _(j):
+        for piece in range(2):
+            along(level, ordered(j), piece).start()
 
     across(level, core, spot).start()
 
@@ -981,6 +982,7 @@
         )
         square_s[at, :, 0:bulk] = squares[0:1, 0:bulk]
         square_s[at, :, bulk : bulk + tail] = squares[0:1, bulk : bulk + tail]
+        squares_s[at, 0] = square_s[at]
 
         @pl.loop(1, n)
         def _(k):
@@ -992,62 +994,6 @@
         up = jnp.clip(jnp.dot(values, e_up_s[...], preferred_element_type=kind), -LIMIT, LIMIT)
         act = ((up + 1.0) * gate * jax.nn.sigmoid(gate * ALPHA)).astype(half_type)
         answer_s[at] = jnp.dot(act, e_down_s[...], preferred_element_type=kind).astype(half_type)
-
-    @pl.loop(0, deep + 1)
-    def _(step):
-        @pl.when(step + 1 < deep)
-        def _():
-            at = ordered(step + 1)
-            for piece in range(2):
-                along(at, 0, piece).wait_recv()
-
-                @pl.when((at < level) & (level + 1 < deep))
-                def _():
-                    along(at, 1, piece).start()
-
-                @pl.when((at > level) & (level > 0))
-                def _():
-                    along(at, 0, piece).start()
-
-                spread_piece(at, piece)
-            across(at, core, spot).start()
-
-        @pl.when(step < deep)
-        def _():
-            at = ordered(step)
-            beside(at, spot_x, 0).wait_recv()
-            relay_a(at, spot_x).start()
-            above(at, spot_y, 1).wait_recv()
-            relay_b(at, spot_y).start()
-            beside(at, spot_x, 1).wait_recv()
-            across(at, core, spot_x).start()
-            above(at, spot_y, 0).wait_recv()
-            across(at, core, spot_y).start()
-
-        @pl.when(step >= 1)
-        def _():
-            at = ordered(step - 1)
-            relay_a(at, spot_d).wait_recv()
-            relay_b(at, spot_d).wait_recv()
-            across(at, core, spot_d).start()
-
-        @pl.when((step >= 2) & (step < deep))
-        def _():
-            run_expert(ordered(step - 2))
-
-        @pl.when(step >= 1)
-        def _():
-            dense_units(ordered(step - 1))
-
-    @pl.loop(deep - 2, deep)
-    def _(step):
-        run_expert(ordered(step))
-
-    informed().wait_recv()
-    shared().wait_recv()
-
-    squares_s[0] = square_s[...]
-    scale_s[...] = lax.rsqrt(jnp.sum(squares_s[...], axis=0) / units_total + EPS)
 
     def columns(line):
         main = to_column(line[:, 0:bulk], same_bulk)
@@ -1064,19 +1010,21 @@
         )
 
     def first(at, k):
+        place_a = lax.rem(row + 1 + k, side)
+        place_b = lax.rem(col + 1 + k, side)
         return (
             reach(
-                pair_s.at[at, k * side + 1 - col, :, 0:cut],
-                first_a.at[at, k],
+                pair_s.at[at, place_a * side + 1 - col, :, 0:cut],
+                first_a.at[at, place_a],
                 back_send.at[0],
-                s1a_recv.at[at],
+                s1a_recv.at[at, lax.rem(place_a + row, side)],
                 near_x,
             ),
             reach(
-                pair_s.at[at, (1 - row) * side + k, :, cut:wide],
-                first_b.at[at, k],
+                pair_s.at[at, (1 - row) * side + place_b, :, cut:wide],
+                first_b.at[at, place_b],
                 back_send.at[0],
-                s1b_recv.at[at],
+                s1b_recv.at[at, lax.rem(place_b + col, side)],
                 near_y,
             ),
         )
@@ -1105,78 +1053,127 @@
             device(at, row, col, core),
         )
 
+    def combine(at):
+        shared(at).wait_recv()
+        dense = jnp.dot(hidden_s[at], d_down_s[...], preferred_element_type=kind)
+        coef = jnp.sum(infos_s[pl.ds(at * members, members)], axis=0)
+        scale = lax.rsqrt(jnp.sum(squares_s[at], axis=0) / units_total + EPS)
+        weight, weight_end = columns(coef)
+        scale, scale_end = columns(scale)
+        twice = branch_col_s[at, :, 0:1]
+        main = weight * answer_s[at, 0:bulk, :].astype(kind)
+        main = main + (scale * twice[0:bulk]) * dense[0:bulk]
+        ends = weight_end * answer_s[at, bulk : bulk + tail, :].astype(kind)
+        ends = ends + (scale_end * twice[bulk:]) * dense[bulk:]
+        part_s[at, :, :, 0:width] = main.astype(half_type).reshape(members, block, width)
+        for piece in range(folds):
+            for tile in range(fold // pair):
+                first_lane = piece * fold + tile * pair
+                for extra in range(spare):
+                    spread_s[tile, pl.ds(piece * spare + extra, members, stride=block), :] = (
+                        ends[
+                            extra * members : (extra + 1) * members,
+                            first_lane : first_lane + pair,
+                        ]
+                    )
+        for tile in range(fold // pair):
+            part_s[at, :, :, width + tile * pair : width + (tile + 1) * pair] = (
+                spread_s[tile].astype(half_type).reshape(members, block, pair)
+            )
+        cross(at).start()
+
+    def join(at):
+        cross(at).wait_recv()
+        mine = part_s[at, pl.ds(core * plane, plane)].astype(kind)
+        pair_s[at] = (mine + joint_s[at].astype(kind)).astype(half_type)
+        for k in range(side):
+            for copy in first(at, k):
+                copy.start()
+
+    def turn(at):
+        for copy in first(at, 0):
+            copy.wait_recv()
+        turned = pair_s[at, spot_y, :, 0:cut].astype(kind) + first_a[at, 1 - row].astype(kind)
+        turn_a[at] = turned.astype(half_type)
+        turned = pair_s[at, spot_x, :, cut:wide].astype(kind) + first_b[at, 1 - col].astype(kind)
+        turn_b[at] = turned.astype(half_type)
+        for copy in second(at):
+            copy.start()
+
+    def settle(at):
+        for copy in first(at, 1):
+            copy.wait_recv()
+        for copy in second(at):
+            copy.wait_recv()
+        total = pair_s[at, spot, :, 0:cut].astype(kind) + first_a[at, row].astype(kind)
+        total = total + second_a[at].astype(kind)
+        level_s[at, :, 0:cut] = total.astype(half_type)
+        total = pair_s[at, spot, :, cut:wide].astype(kind) + first_b[at, col].astype(kind)
+        total = total + second_b[at].astype(kind)
+        level_s[at, :, cut:wide] = total.astype(half_type)
+
+        @pl.when(at != level)
+        def _():
+            home_to(at).start()
+
+    def native(at):
+        for piece in range(2):
+            along(at, 0, piece).wait_recv()
+            spread_piece(at, piece)
+        across(at, core, spot).start()
+
+    def relay(at):
+        beside(at, spot_x, 0).wait_recv()
+        relay_a(at, spot_x).start()
+        above(at, spot_y, 1).wait_recv()
+        relay_b(at, spot_y).start()
+        beside(at, spot_x, 1).wait_recv()
+        across(at, core, spot_x).start()
+        above(at, spot_y, 0).wait_recv()
+        across(at, core, spot_y).start()
+
+    def corner(at):
+        relay_a(at, spot_d).wait_recv()
+        relay_b(at, spot_d).wait_recv()
+        across(at, core, spot_d).start()
+
+    def at_step(step, start, stop, act, lag, order):
+        @pl.when((step >= start) & (step < stop))
+        def _():
+            act(order(step - lag))
+
+    relay(ordered(0))
+    native(ordered(1))
+    corner(ordered(0))
+    native(ordered(2))
+    relay(ordered(1))
+    native(ordered(3))
+    dense_units(ordered(0))
+    relay(ordered(2))
+    corner(ordered(1))
+    run_expert(ordered(0))
+    relay(ordered(3))
+    corner(ordered(2))
+    dense_units(ordered(1))
+    dense_units(ordered(2))
+    corner(ordered(3))
+    run_expert(ordered(1))
+    dense_units(ordered(3))
+    run_expert(ordered(2))
+    run_expert(ordered(3))
+
+    informed().wait_recv()
+
     @pl.loop(0, deep + 3)
     def _(step):
-        @pl.when(step < deep)
-        def _():
-            at = ordered(deep - 1 - step)
-            dense = jnp.dot(hidden_s[at], d_down_s[...], preferred_element_type=kind)
-            coef = jnp.sum(infos_s[pl.ds(at * members, members)], axis=0)
-            weight, weight_end = columns(coef)
-            scale, scale_end = columns(scale_s[at])
-            twice = branch_col_s[at, :, 0:1]
-            main = weight * answer_s[at, 0:bulk, :].astype(kind)
-            main = main + (scale * twice[0:bulk]) * dense[0:bulk]
-            ends = weight_end * answer_s[at, bulk : bulk + tail, :].astype(kind)
-            ends = ends + (scale_end * twice[bulk:]) * dense[bulk:]
-            part_s[at, :, :, 0:width] = main.astype(half_type).reshape(members, block, width)
-            for piece in range(folds):
-                for tile in range(fold // pair):
-                    first_lane = piece * fold + tile * pair
-                    for extra in range(spare):
-                        spread_s[tile, pl.ds(piece * spare + extra, members, stride=block), :] = (
-                            ends[
-                                extra * members : (extra + 1) * members,
-                                first_lane : first_lane + pair,
-                            ]
-                        )
-            for tile in range(fold // pair):
-                part_s[at, :, :, width + tile * pair : width + (tile + 1) * pair] = (
-                    spread_s[tile].astype(half_type).reshape(members, block, pair)
-                )
-            cross(at).start()
-
-        @pl.when((step >= 1) & (step < deep + 1))
-        def _():
-            at = ordered(deep - step)
-            cross(at).wait_recv()
-            mine = part_s[at, pl.ds(core * plane, plane)].astype(kind)
-            pair_s[at] = (mine + joint_s[at].astype(kind)).astype(half_type)
-            for k in range(side):
-                for copy in first(at, k):
-                    copy.start()
-
-        @pl.when((step >= 2) & (step < deep + 2))
-        def _():
-            at = ordered(deep + 1 - step)
-            for here, sem in ((first_a.at[at], s1a_recv.at[at]), (first_b.at[at], s1b_recv.at[at])):
-                reach(here, here, back_send.at[0], sem, other).wait_recv()
-            turned = pair_s[at, spot_y, :, 0:cut].astype(kind) + first_a[at, 1 - row].astype(kind)
-            turn_a[at] = turned.astype(half_type)
-            turned = pair_s[at, spot_x, :, cut:wide].astype(kind) + first_b[at, 1 - col].astype(kind)
-            turn_b[at] = turned.astype(half_type)
-            for copy in second(at):
-                copy.start()
-
-        @pl.when(step >= 3)
-        def _():
-            at = ordered(deep + 2 - step)
-            for copy in second(at):
-                copy.wait_recv()
-            total = pair_s[at, spot, :, 0:cut].astype(kind) + first_a[at, row].astype(kind)
-            total = total + second_a[at].astype(kind)
-            level_s[at, :, 0:cut] = total.astype(half_type)
-            total = pair_s[at, spot, :, cut:wide].astype(kind) + first_b[at, col].astype(kind)
-            total = total + second_b[at].astype(kind)
-            level_s[at, :, cut:wide] = total.astype(half_type)
-
-            @pl.when(step < deep + 2)
-            def _():
-                home_to(at).start()
+        at_step(step, 0, deep, combine, 0, returned)
+        at_step(step, 1, deep + 1, join, 1, returned)
+        at_step(step, 2, deep + 2, turn, 2, returned)
+        at_step(step, 3, deep + 3, settle, 3, returned)
 
     total = level_s[level].astype(kind)
-    for j in range(1, deep):
-        at = ordered(j)
+    for j in range(deep - 1):
+        at = returned(j)
         home_from(at).wait_recv()
         total = total + levels_s[at].astype(kind)
     out[0:block, :] = (mixed_s[0:block, :] + total[:, 0:width]).astype(half_type)
@@ -1186,22 +1183,11 @@
         ends = mixed_s[block:seqs, lanes] + fold_s[pl.ds(part * spare, spare), :]
         out[block:seqs, lanes] = ends.astype(half_type)
 
-    @pl.loop(0, deep)
-    def _(at):
-        whole = rows_s.at[slot(at, core, spot)]
-
-        @pl.when((at <= level) & (level + 1 < deep))
-        def _():
-            reach(whole, whole, z_send.at[1, at], z_send.at[1, at], other).wait_send()
-
-        @pl.when((at >= level) & (level > 0))
-        def _():
-            reach(whole, whole, z_send.at[0, at], z_send.at[0, at], other).wait_send()
-
-    sent(chips + 3 * deep, rows_send.at[0]).wait_send()
+    sent(chips + 4 * deep - 1, rows_send.at[0]).wait_send()
     sent(chips + 4 * deep - 1, back_send.at[0]).wait_send()
     informed().wait_send()
-    shared().wait_send()
+    every = squares_s.at[:, pl.ds(1, n - 1)]
+    reach(every, every, q_send.at[0], q_recv.at[0], other).wait_send()
 
 
 def fast(n, deep, arrays, units_total):
@@ -1268,10 +1254,9 @@
         vmem((deep, bulk + tail, local), half_type),
         vmem((deep, bulk + tail, pair), kind),
         vmem((deep, 1, 2 * bulk), kind),
-        vmem((n, deep, 1, 2 * bulk), kind),
+        vmem((deep, n, 1, 2 * bulk), kind),
         vmem((n, 1, 2 * bulk), kind),
         vmem((n, 1, 2 * bulk), kind),
-        vmem((deep, 1, 2 * bulk), kind),
         vmem((deep, bulk + tail, width), half_type),
         vmem((deep, members, block, wide), half_type),
         vmem((deep, plane, block, wide), half_type),
@@ -1287,7 +1272,6 @@
         dma((21,)),
         dma((2, groups)),
         dma((2, deep)),
-        dma((2, deep)),
         dma((1,)),
         dma((2, deep)),
         dma((2, deep)),
@@ -1297,11 +1281,11 @@
         dma((1,)),
         dma((1,)),
         dma((1,)),
-        dma((1,)),
+        dma((deep,)),
         dma((1,)),
         dma((deep,)),
-        dma((deep,)),
-        dma((deep,)),
+        dma((deep, 2)),
+        dma((deep, 2)),
         dma((deep,)),
         dma((deep,)),
         dma((deep,)),

time: 56.3 us -> 52.6 us (0.934)
  Pallas kernels: 54.6 us -> 50.9 us
    pallas_call x1, Pallas kernels: 54.6 us -> 50.9 us  [fast(): pl.pallas_call(functools.partial(fast_body, units_total), out_shape=jax.S...]
where the time goes in v3:
time: 52.6 us; the launch traced here: 52.5 us
  Pallas kernels  50.9 us (97%)
  local copies, waits for them, and re-layouts  1.54 us (3%)
    pallas_call x1, Pallas kernels, fast(): pl.pallas_call(functools.partial(fast_body, units_total), out_shape=jax.S...  50.9 us
    unnamed x1, local copies, waits for them, and re-layouts  1.54 us

profile of v3, /device:TPU:0, one launch (start us, length us, event | category | flops | bytes accessed | tf_op | source)
XLA Modules:
  0.0 52.5 jit_solution(13764639982773174721)
XLA Ops:
  0.0 50.9 %layer.1 = bf16[18,2048]{1,0:T(8,128)(2,1)} custom-call(bf16[18,2048]{1,0:T(8,128)(2,1)} %tokens_h.1, f32[1,2048]{1,0:T(1,128)} %bitcast.10, bf16[2048,512]{1,0:T(8,128)(2,1)} %w_query_h.1, bf16[2048,128]{1,0:T(8,128)(2,1)} %w_key_h.1, bf16[2048,128]{1,0:T(8,128)(2,1)} %w_value_h.1, bf16[8,2048]{1,0:T(8,128)(2,1)} %bitcast.8, f32[1,8]{1,0:T(1,128)} %bitcast.15, ...), custom_call_target="tpu_custom_call" | custom-call | tf_op jit(solution)/shard_map/layer/pallas_call | solution.py:1293
  50.9 1.5 %copy.25 = bf16[18,2048]{1,0:T(8,128)(2,1)} copy(bf16[18,2048]{1,0:T(8,128)(2,1)} %layer.1) | data formatting | bytes 147456

commit v4 on v3

--- a/solution.py
+++ b/solution.py
@@ -571,8 +571,7 @@
     gain_next_s,
     ids_s,
     weights_s,
-    e_gate_s,
-    e_up_s,
+    e_in_s,
     e_down_s,
     d_in_s,
     d_down_s,
@@ -687,8 +686,8 @@
         (d_up_h, d_in_s.at[:, pair : 2 * pair]),
         (d_gain_h, d_gain_s),
         (branch_h, branch_s),
-        (e_gate_h.at[0], e_gate_s),
-        (e_up_h.at[0], e_up_s),
+        (e_gate_h.at[0], e_in_s.at[:, 0 : e_in_s.shape[1] // 2]),
+        (e_up_h.at[0], e_in_s.at[:, e_in_s.shape[1] // 2 :]),
         (e_down_h.at[0], e_down_s),
         (d_down_h, d_down_s),
     ]
@@ -798,7 +797,14 @@
         for item in range(batch):
             seq = at * batch + item
             part = slice(item * HEADS, (item + 1) * HEADS)
-            result = jnp.dot(share[part], values_s[seq], preferred_element_type=kind)
+            if item % 2 == 0:
+                paired = jnp.dot(
+                    share[item * HEADS : (item + 2) * HEADS],
+                    jnp.concatenate([values_s[seq], values_s[seq + 1]], axis=1),
+                    preferred_element_type=kind,
+                )
+            odd = item % 2
+            result = paired[odd * HEADS : (odd + 1) * HEADS, odd * pair : (odd + 1) * pair]
             result = result + own_share[part] * value_s[pl.ds(seq, 1), :]
             heads_s[pl.ds(pl.multiple_of(seq * HEADS, HEADS), HEADS), :] = result
 
@@ -889,20 +895,15 @@
         here = rows_s.at[pl.ds(slot(at, 1 - core, 0), plane)]
         return reach(here, here, rows_send.at[0], f_recv.at[at], other)
 
-    balance = jnp.minimum(level, deep - 1 - level)
-    lean = jnp.where(2 * level < deep - 1, 1, -1)
+    def paired(j):
+        high = lax.rem(level // 2 + j // 2, 2)
+        return high * 2 + lax.rem(level + j, 2)
 
     def ordered(j):
-        paired = jnp.where(lax.rem(j, 2) == 1, -1, 1) * ((j + 1) // 2)
-        single = lean * (j - balance)
-        return level + jnp.where(j <= 2 * balance, paired, single)
-
-    rank = jnp.where(level == 0, deep - 2, jnp.where(level == deep - 1, level, level - 1))
+        return paired(j)
 
     def returned(j):
-        k = j + jnp.where(j >= rank, 1, 0)
-        k = jnp.where(k < deep - 2, k + 1, jnp.where(k == deep - 2, 0, deep - 1))
-        return jnp.where(j == deep - 1, level, k)
+        return paired(deep - 1 - j)
 
     def share(k, at):
         return reach(
@@ -973,25 +974,21 @@
         gate, up = both[:, 0:pair], both[:, pair : 2 * pair]
         units = (gate * jax.nn.sigmoid(gate) * up).astype(half_type).astype(kind)
         hidden_s[at] = (units * d_gain_s[pl.ds(me, 1), :]).astype(half_type)
-        squares = lax.dot_general(
-            ones,
-            units * units,
-            (((1,), (1,)), ((), ())),
-            preferred_element_type=kind,
-            precision=exact,
-        )
-        square_s[at, :, 0:bulk] = squares[0:1, 0:bulk]
-        square_s[at, :, bulk : bulk + tail] = squares[0:1, bulk : bulk + tail]
+        squares = jnp.sum(units * units, axis=1, keepdims=True)
+        square_s[at, :, 0:bulk] = to_row(squares[0:bulk], same_bulk)
+        ends = jnp.where(tail_at == tail_of, squares[bulk:], 0.0)
+        square_s[at, :, bulk : 2 * bulk] = jnp.sum(ends, axis=0, keepdims=True)
         squares_s[at, 0] = square_s[at]
 
-        @pl.loop(1, n)
-        def _(k):
+        for k in range(1, n):
             share(k, at).start()
 
     def run_expert(at):
         values = x_s[at]
-        gate = jnp.minimum(jnp.dot(values, e_gate_s[...], preferred_element_type=kind), LIMIT)
-        up = jnp.clip(jnp.dot(values, e_up_s[...], preferred_element_type=kind), -LIMIT, LIMIT)
+        both = jnp.dot(values, e_in_s[...], preferred_element_type=kind)
+        ff = e_in_s.shape[1] // 2
+        gate = jnp.minimum(both[:, 0:ff], LIMIT)
+        up = jnp.clip(both[:, ff : 2 * ff], -LIMIT, LIMIT)
         act = ((up + 1.0) * gate * jax.nn.sigmoid(gate * ALPHA)).astype(half_type)
         answer_s[at] = jnp.dot(act, e_down_s[...], preferred_element_type=kind).astype(half_type)
 
@@ -1155,9 +1152,9 @@
     relay(ordered(3))
     corner(ordered(2))
     dense_units(ordered(1))
+    run_expert(ordered(1))
+    corner(ordered(3))
     dense_units(ordered(2))
-    corner(ordered(3))
-    run_expert(ordered(1))
     dense_units(ordered(3))
     run_expert(ordered(2))
     run_expert(ordered(3))
@@ -1234,8 +1231,7 @@
         vmem((1, width), kind),
         vmem((TOPK, seqs), jnp.int32),
         vmem((TOPK, seqs), kind),
-        vmem((width, hidden), half_type),
-        vmem((width, hidden), half_type),
+        vmem((width, 2 * hidden), half_type),
         vmem((hidden, width), half_type),
         vmem((width, 2 * local), half_type),
         vmem((local, width), half_type),

time: 52.6 us -> 50.7 us (0.964)
  Pallas kernels: 50.9 us -> 49 us
    pallas_call x1, Pallas kernels: 50.9 us -> 49 us  [fast(): pl.pallas_call(functools.partial(fast_body, units_total), out_shape=jax.S...]
where the time goes in v4:
time: 50.7 us; the launch traced here: 50.6 us
  Pallas kernels  49 us (97%)
  local copies, waits for them, and re-layouts  1.54 us (3%)
    pallas_call x1, Pallas kernels, fast(): pl.pallas_call(functools.partial(fast_body, units_total), out_shape=jax.S...  49 us
    unnamed x1, local copies, waits for them, and re-layouts  1.54 us

profile of v4, /device:TPU:0, one launch (start us, length us, event | category | flops | bytes accessed | tf_op | source)
XLA Modules:
  0.0 50.6 jit_solution(1375994167475150693)
XLA Ops:
  0.0 49.0 %layer.1 = bf16[18,2048]{1,0:T(8,128)(2,1)} custom-call(bf16[18,2048]{1,0:T(8,128)(2,1)} %tokens_h.1, f32[1,2048]{1,0:T(1,128)} %bitcast.10, bf16[2048,512]{1,0:T(8,128)(2,1)} %w_query_h.1, bf16[2048,128]{1,0:T(8,128)(2,1)} %w_key_h.1, bf16[2048,128]{1,0:T(8,128)(2,1)} %w_value_h.1, bf16[8,2048]{1,0:T(8,128)(2,1)} %bitcast.8, f32[1,8]{1,0:T(1,128)} %bitcast.15, ...), custom_call_target="tpu_custom_call" | custom-call | tf_op jit(solution)/shard_map/layer/pallas_call | solution.py:1289
  49.0 1.5 %copy.25 = bf16[18,2048]{1,0:T(8,128)(2,1)} copy(bf16[18,2048]{1,0:T(8,128)(2,1)} %layer.1) | data formatting | bytes 147456
